TPU v7x, 256 devices: a 4x2x16 block of a 4x16x16 slice. The times are simulated.
256 devices in a mesh: grp: 2 (over y), sp: 32 (over z, core), tp: 4 (over x).
Axes of the slice: x: 4, y: 2, z: 16, core: 2. Of those that a mesh axis runs over, the one named last changes fastest.
The devices are a block of a 4x16x16 slice.
Arguments:
- query_rows: bfloat16 [32768, 512], P(('grp', 'sp'), 'tp'), parts along dimension 0, may hold values from -12 to 12
- key_rows: bfloat16 [32768, 512], P(('grp', 'sp'), 'tp'), parts along dimension 0, may hold values from -12 to 12
- value_rows: bfloat16 [32768, 512], P(('grp', 'sp'), 'tp'), parts along dimension 0, may hold values from -12 to 12
- residual: bfloat16 [32768, 2048], P(('grp', 'sp', 'tp')), parts along dimension 0, may hold values from -6 to 6
- output_weight: bfloat16 [512, 2048], P('tp'), may hold values from -0.25 to 0.25
- first_gain: float32 [2048], replicated, may hold values from 0.1 to 1.9
- first_bias: float32 [2048], replicated, may hold values from -3 to 3
- expert_ids: int32 [32768, 4], P(('grp', 'sp', 'tp')), parts along dimension 0, may hold values from 0 to 127, all different within a row; in each aligned block of 128 rows (0 to 127, 128 to 255, ...) at most 6 rows name the same one
- expert_share: float32 [32768, 4], P(('grp', 'sp', 'tp')), parts along dimension 0, may hold values from 0.3 to 1.2
- gate_weight: bfloat16 [128, 2048, 256], P(('sp', 'tp')), may hold values from -0.125 to 0.125
- up_weight: bfloat16 [128, 2048, 256], P(('sp', 'tp')), may hold values from -0.125 to 0.125
- down_weight: bfloat16 [128, 256, 2048], P(('sp', 'tp')), may hold values from -0.375 to 0.375
- shared_gate: bfloat16 [2048, 512], replicated, may hold values from -0.125 to 0.125
- shared_up: bfloat16 [2048, 512], replicated, may hold values from -0.125 to 0.125
- shared_down: bfloat16 [512, 2048], replicated, may hold values from -0.25 to 0.25
- second_gain: float32 [2048], replicated, may hold values from 0.1 to 1.9
- second_bias: float32 [2048], replicated, may hold values from -3 to 3
Outputs:
- layer_out: bfloat16 [32768, 2048], P(('grp', 'sp', 'tp')), parts along dimension 0
There are 2 independent parts, one for each index of `grp`. A program takes and returns all parts, laid end to end along the dimension named above; an argument that names none is the same for every part. Nothing has to cross between parts.
Inputs may be any that keep to these rules, and one draw needn't show every extreme that they name: `expert_ids`: each row names 4 different experts. Among the rows of one device (aligned blocks of 128 rows) no expert is named by more than 6 rows, a bound that some block reaches.
All inputs are finite; a program needn't handle non-finite values.
Results may differ from a plain program's by a relative error of at most 0.012.
Values may be sent and summed in bfloat16 or wider, within the bound.
A program may use at most 128 MiB of HBM per device.

v0:
```python
import jax
import jax.numpy as jnp
from jax import lax
from jax.sharding import PartitionSpec as P

HEAD_DIM = 128
KBLK = 128


NORM_EPS = 1e-05


def in_one_piece(arrays, axis, dim, along):
    both = jnp.concatenate(arrays, axis=along)
    filled, at, gathered = (lax.all_gather(both, axis, axis=dim, tiled=True), 0, [])
    for a in arrays:
        gathered.append(lax.slice_in_dim(filled, at, at + a.shape[along], axis=along))
        at += a.shape[along]
    return tuple(gathered)


def sent_to_all(array, axis):
    copies = jnp.broadcast_to(array, (lax.axis_size(axis), *array.shape))
    return lax.all_to_all(copies, axis, split_axis=0, concat_axis=0, tiled=True)


def laid_out(tiles, dim):
    tiles = jnp.moveaxis(tiles, 0, dim)
    lengths = tiles.shape
    return tiles.reshape(*lengths[:dim], lengths[dim] * lengths[dim + 1], *lengths[dim + 2 :])


def collect(array, axis, dim):
    tiles = sent_to_all(array, axis)
    return laid_out(tiles, dim)


def layer_norm(summed, gains, offset):
    average = jnp.mean(summed, axis=-1, keepdims=True)
    centred = summed - average
    spread = jnp.mean(centred * centred, axis=-1, keepdims=True)
    return centred * lax.rsqrt(spread + NORM_EPS) * gains + offset


def stick_local(query_rows, key_all, value_all, seq_index):
    shard_len = query_rows.shape[0]
    heads_here = query_rows.shape[1] // HEAD_DIM
    step_len = 2 * shard_len
    blocks_per = step_len // KBLK
    scale = HEAD_DIM ** (-0.5)
    queries = query_rows.reshape(shard_len, heads_here, HEAD_DIM)
    query_pos = seq_index * shard_len + jnp.arange(shard_len, dtype=jnp.int32)
    visits = seq_index // 2 + 1
    upper = (jnp.arange(KBLK)[:, None] >= jnp.arange(KBLK)[None, :]).astype(jnp.float32)

    def visit(visit_no, carry):
        summed, behind = carry
        chosen = visits - 1 - visit_no
        first_key = chosen * step_len
        key_block = lax.dynamic_slice_in_dim(key_all, first_key, step_len, 0).reshape(
            step_len, heads_here, HEAD_DIM
        )
        value_block = lax.dynamic_slice_in_dim(value_all, first_key, step_len, 0).reshape(
            blocks_per, KBLK, heads_here, HEAD_DIM
        )
        key_pos = (first_key + jnp.arange(step_len, dtype=jnp.int32)).reshape(blocks_per, KBLK)
        score = (
            jnp.einsum("qhd,khd->qhk", queries, key_block, preferred_element_type=jnp.float32)
            * scale
        )
        score = score.reshape(shard_len, heads_here, blocks_per, KBLK)
        usable = key_pos[None, None, :, :] < query_pos[:, None, None, None]
        spent = jnp.where(usable, jax.nn.softplus(score), 0.0)
        inside = jnp.dot(spent.reshape(-1, KBLK), upper).reshape(spent.shape)
        totals = inside[..., 0]
        weight = jnp.where(usable, jnp.exp(score - inside), 0.0).astype(jnp.bfloat16)
        pieces = jnp.einsum(
            "qhbk,bkhd->qhbd", weight, value_block, preferred_element_type=jnp.float32
        )
        block_running = jnp.cumsum(totals, axis=-1)
        step_total = block_running[..., -1]
        beyond = step_total[..., None] - block_running
        factor = jnp.exp(-(behind[..., None] + beyond))
        summed = summed + jnp.sum(pieces * factor[..., None], axis=2)
        return (summed, behind + step_total)

    initial = (
        jnp.zeros((shard_len, heads_here, HEAD_DIM), jnp.float32),
        jnp.zeros((shard_len, heads_here), jnp.float32),
    )
    summed, _ = lax.fori_loop(0, visits, visit, initial)
    return summed.reshape(shard_len, heads_here * HEAD_DIM).astype(jnp.bfloat16)


def local(
    query_rows,
    key_rows,
    value_rows,
    residual,
    output_weight,
    first_gain,
    first_bias,
    expert_ids,
    expert_share,
    gate_weight,
    up_weight,
    down_weight,
    shared_gate,
    shared_up,
    shared_down,
    second_gain,
    second_bias,
):
    seq_index = lax.axis_index("sp")
    key_all, value_all = in_one_piece((key_rows, value_rows), "sp", 0, 1)
    attended = stick_local(query_rows, key_all, value_all, seq_index)
    tokens_here = residual.shape[0]
    width = residual.shape[1]
    by_token = lax.all_to_all(attended, "tp", split_axis=0, concat_axis=1, tiled=True)
    mixed = jnp.dot(by_token, collect(output_weight, "tp", 0), preferred_element_type=jnp.float32)
    normed = layer_norm(residual.astype(jnp.float32) + mixed, first_gain, first_bias).astype(
        jnp.bfloat16
    )
    top_count = expert_ids.shape[1]
    pair_count = tokens_here * top_count
    experts = lax.axis_size("sp") * lax.axis_size("tp")
    capacity = max(2, 3 * pair_count // (2 * experts))
    flat_ids = expert_ids.reshape(pair_count)
    one_hot = (flat_ids[:, None] == jnp.arange(experts, dtype=jnp.int32)[None, :]).astype(
        jnp.bfloat16
    )
    earlier_mask = (jnp.arange(pair_count)[:, None] > jnp.arange(pair_count)[None, :]).astype(
        jnp.bfloat16
    )
    before = jnp.dot(earlier_mask, one_hot, preferred_element_type=jnp.float32)
    ranked = jnp.sum(before * one_hot, axis=1).astype(jnp.int32)
    slot_ids = flat_ids * capacity + ranked
    selector = jnp.any(
        slot_ids.reshape(tokens_here, top_count)[None, :, :]
        == jnp.arange(experts * capacity, dtype=jnp.int32)[:, None, None],
        axis=2,
    )
    outgoing = jnp.dot(selector.astype(jnp.bfloat16), normed, preferred_element_type=jnp.float32)
    outgoing = outgoing.astype(jnp.bfloat16).reshape(experts, capacity, width)
    slot_rows = lax.all_to_all(outgoing, ("sp", "tp"), split_axis=0, concat_axis=0, tiled=True)
    flat_rows = slot_rows.reshape(-1, width)
    gate_act = jnp.dot(flat_rows, gate_weight[0], preferred_element_type=jnp.float32)
    up_act = jnp.dot(flat_rows, up_weight[0], preferred_element_type=jnp.float32)
    hidden = (jax.nn.silu(gate_act) * up_act).astype(jnp.bfloat16)
    produced = jnp.dot(hidden, down_weight[0], preferred_element_type=jnp.float32).astype(
        jnp.bfloat16
    )
    results = produced.reshape(slot_rows.shape)
    returned = lax.all_to_all(results, ("sp", "tp"), split_axis=0, concat_axis=0, tiled=True)
    flat_back = returned.reshape(experts * capacity, width)
    picked = jnp.take(flat_back, slot_ids, axis=0).reshape(tokens_here, top_count, width)
    routed = jnp.sum(picked.astype(jnp.float32) * expert_share[:, :, None], axis=1)
    gate_act = jnp.dot(normed, shared_gate, preferred_element_type=jnp.float32)
    up_act = jnp.dot(normed, shared_up, preferred_element_type=jnp.float32)
    shared_hidden = (jax.nn.silu(gate_act) * up_act).astype(jnp.bfloat16)
    shared_out = jnp.dot(shared_hidden, shared_down, preferred_element_type=jnp.float32)
    final = layer_norm(normed.astype(jnp.float32) + routed + shared_out, second_gain, second_bias)
    return final.astype(jnp.bfloat16)


def solution(mesh):
    return jax.shard_map(
        local,
        mesh=mesh,
        in_specs=(
            P(("grp", "sp"), "tp"),
            P(("grp", "sp"), "tp"),
            P(("grp", "sp"), "tp"),
            P(("grp", "sp", "tp"), None),
            P("tp", None),
            P(),
            P(),
            P(("grp", "sp", "tp"), None),
            P(("grp", "sp", "tp"), None),
            P(("sp", "tp"), None, None),
            P(("sp", "tp"), None, None),
            P(("sp", "tp"), None, None),
            P(),
            P(),
            P(),
            P(),
            P(),
        ),
        out_specs=P(("grp", "sp", "tp"), None),
        check_vma=False,
    )
```

profile of v0, /device:TPU:33, one launch (start us, length us, event | category | flops | bytes accessed | tf_op | source)
XLA Modules:
  0.0 933.1 jit_solution(9294784564449240976)
XLA Ops:
  11.1 5.2 all-to-all-start.1
  17.1 84.1 %all-gather.2.cloned.1.call-done = bf16[16384,256]{1,0:T(8,128)(2,1)} async-done(((bf16[512,256]{1,0:T(8,128)(2,1)}), bf16[16384,256]{1,0:T(8,128)(2,1)}) %all-gather.2.cloned.1.call-update) | async-done | bytes 8388624 | tf_op jit(solution)/shard_map/all_gather | solution.py:15
  101.2 5.7 fusion.62
  106.9 21.9 %while.15 = (s32[]{:T(128)}, f32[512,1,128]{0,2,1:T(8,128)S(1)}, f32[512,1]{0,1:T(1,128)S(1)}, s32[]{:T(128)}, s32[]{:T(128)}, /*index=5*/bf16[16384,128]{1,0:T(...) while((s32[]{:T(128)}, f32[512,1,128]{0,2,1:T(8,128)S(1)}, ...), condition=%wide.region_3.4_spmd.clone, body=%wide.region_0.3_spmd.clone.sunk | while | flops 410595328 | bytes 25510100 | solution.py:91
  107.0 2.8 convolution_multiply_fusion.5
  109.8 2.9 copy.79
  115.7 3.7 fusion.92
  121.6 2.9 copy.78
  125.5 3.2 fusion.94
  129.6 4.0 all-to-all-start
  133.9 4.6 all-to-all-done
  143.8 6.3 reshape.271
  150.0 524.6 %all_to_all.28 = bf16[128,6,2048]{2,1,0:T(8,128)(2,1)} all-to-all(bf16[128,6,2048]{2,1,0:T(8,128)(2,1)} %reshape.271), channel_id=1, replica_groups=mesh['grp'=2,'sp'=32,'tp'=4] {'sp','tp'}, dimensions={0} | all-to-all | bytes 6291456 | tf_op jit(solution)/shard_map/all_to_all | solution.py:145
  674.6 6.3 reshape.272
  681.0 4.0 fusion.41
  685.0 7.8 convolution_convert_fusion
  692.8 6.3 reshape.273
  699.1 11.1 %all-to-all-start.3 = ((bf16[128,6,2048]{2,1,0:T(8,128)(2,1)}), bf16[128,6,2048]{2,1,0:T(8,128)(2,1)}, u32[]{:S(2)}, u32[]{:S(2)}) async-start(bf16[128,6,2048]{2,1,0:T(8,128)(2,1)} %reshape.273), calls=%async_computation.3 | async-start | bytes 8388608 | tf_op jit(solution)/shard_map/all_to_all | solution.py:154
  712.7 184.4 %all-to-all-done.3 = bf16[128,6,2048]{2,1,0:T(8,128)(2,1)} async-done(((bf16[128,6,2048]{2,1,0:T(8,128)(2,1)}), bf16[128,6,2048]{2,1,0:T(8,128)(2,1)}, u32[]{:S(2)}, u32[]{:S(2)}) %all-to-all-start.3) | async-done | bytes 3145760 | tf_op jit(solution)/shard_map/all_to_all | solution.py:154
  897.1 6.3 reshape.274
  903.4 7.6 gather_fusion
  911.0 4.1 gather.7
  915.1 6.6 multiply_reduce_fusion
  921.7 3.1 fusion.64
  (66 shorter events, 21.7 us)
Async XLA Ops:
  6.5 915.2 %copy-start = (bf16[512,2048]{1,0:T(8,128)(2,1)S(1)}, bf16[512,2048]{1,0:T(8,128)(2,1)}, u32[]{:S(2)}) copy-start(bf16[512,2048]{1,0:T(8,128)(2,1)} %param.33) | copy-start | bytes 6291460
  6.6 94.6 %all-gather.2.cloned.1.call-start = ((), (), s32[]{:S(2)}) async-start(), calls=%async_computation.4 | async-start | bytes 8650752 | tf_op jit(solution)/shard_map/all_gather | solution.py:15
  11.1 5.3 copy-start.4
  11.1 118.6 %all-to-all-start.1 = ((bf16[4,128,2048]{2,1,0:T(8,128)(2,1)}), bf16[4,128,2048]{2,1,0:T(8,128)(2,1)}, u32[]{:S(2)}, u32[]{:S(2)}) async-start(bf16[4,128,2048]{2,1,0:T(8,128)(2,1)} %broadcast_in_dim.21), calls=%async_computation.1 | async-start | bytes 4194304 | tf_op jit(solution)/shard_map/all_to_all | solution.py:24
  17.1 89.8 %copy-start.2 = (bf16[512,128]{1,0:T(8,128)(2,1)S(1)}, bf16[512,128]{1,0:T(8,128)(2,1)}, u32[]{:S(2)}) copy-start(bf16[512,128]{1,0:T(8,128)(2,1)} %param.19) | copy-start | bytes 393220
  106.9 31.5 %copy-start.3 = (bf16[128,2048]{1,0:T(8,128)(2,1)S(1)}, bf16[128,2048]{1,0:T(8,128)(2,1)}, u32[]{:S(2)}) copy-start(bf16[128,2048]{1,0:T(8,128)(2,1)} %param.22) | copy-start | bytes 1572868
  129.6 8.8 all-to-all-start
  133.8 7.0 copy-start.5
  133.8 7.0 copy-start.6
  141.1 569.6 %copy-start.1 = (bf16[128,2048]{1,0:T(8,128)(2,1)}, bf16[128,2048]{1,0:T(8,128)(2,1)S(1)}, u32[]{:S(2)}) copy-start(bf16[128,2048]{1,0:T(8,128)(2,1)S(1)} %add_convert_fusion.1) | copy-start | bytes 1572868
  699.1 11.5 %copy-start.9 = (f32[128,4]{0,1:T(4,128)S(1)}, f32[128,4]{0,1:T(4,128)}, u32[]{:S(2)}) copy-start(f32[128,4]{0,1:T(4,128)} %param.27) | copy-start | bytes 6148
  699.1 198.0 %all-to-all-start.3 = ((bf16[128,6,2048]{2,1,0:T(8,128)(2,1)}), bf16[128,6,2048]{2,1,0:T(8,128)(2,1)}, u32[]{:S(2)}, u32[]{:S(2)}) async-start(bf16[128,6,2048]{2,1,0:T(8,128)(2,1)} %reshape.273), calls=%async_computation.3 | async-start | bytes 8388608 | tf_op jit(solution)/shard_map/all_to_all | solution.py:154
  921.7 3.4 copy-start.7
  921.7 3.4 copy-start.8
Sparse Core Ops, SparseCore 0:
  9.2 91.9 all-gather.1
where the time goes:
time: 938 us; the launch traced here: 933 us
  blocking collectives  525 us (56%)
  waiting for transfers between devices  273 us (29%)
  local copies, waits for them, and re-layouts  58.8 us (6%)
  matrix products  31.8 us (3%)
  starting transfers between devices  20.3 us (2%)
  between operations  13.6 us (1%)
  other arithmetic  10.7 us (1%)
    all_to_all x1, blocking collectives, local(): lax.all_to_all(outgoing, ('sp', 'tp'), split_axis=0, concat_axis=0, tiled...  525 us
    all_to_all x1, waiting for transfers between devices, local(): lax.all_to_all(results, ('sp', 'tp'), split_axis=0, concat_axis=0, tiled=...  184 us
    all_gather x1, waiting for transfers between devices, in_one_piece(): lax.all_gather(both, axis, axis=dim, tiled=True)  84.1 us
  transfers between devices with their start and end apart: 4, of which 3 were waited for; matrix products, arithmetic and copies ran while one was open for 4% of the time, Pallas kernels for 0%

commit v1 on v0

v1 whole, which is shorter than its diff:
```python
import functools

import jax
import jax.numpy as jnp
from jax import lax
from jax.experimental import pallas as pl
from jax.experimental.pallas import tpu as pltpu
from jax.sharding import PartitionSpec as P

HEAD_DIM = 128
KBLK = 128
NORM_EPS = 1e-05
LOG2E = 1.4426950408889634
MESH = pl.DeviceIdType.MESH
SLOTS = 8
BF16 = jnp.bfloat16
F32 = jnp.float32


def at_sp(sp):
    return {"sp": sp}


def place():
    sp = lax.axis_index("sp")
    return sp, sp // 2, sp % 2, lax.axis_index("tp")


def greet(devices):
    barrier = pltpu.get_barrier_semaphore()
    for device in devices:
        pl.semaphore_signal(barrier, inc=1, device_id=device, device_id_type=MESH)
    pl.semaphore_wait(barrier, len(devices))


def remote(src, dst, send_sem, recv_sem, device):
    return pltpu.make_async_remote_copy(
        src_ref=src,
        dst_ref=dst,
        send_sem=send_sem,
        recv_sem=recv_sem,
        device_id=device,
        device_id_type=MESH,
    )


def attention_kernel(
    nz,
    nx,
    q_ref,
    k_ref,
    v_ref,
    wo_ref,
    aux_ref,
    out_ref,
    wo_out,
    aux_out,
    kv,
    acc,
    behind,
    far,
    ring_send,
    ring_recv,
    pair_send,
    pair_recv,
    own_send,
    own_recv,
    aux_send,
    aux_recv,
    wo_send,
    wo_recv,
):
    sp, z, core, x = place()
    rows = q_ref.shape[0]
    half = rows // 2
    nsp = 2 * nz
    far_hop = nz // 2 - 1
    hop_to = (
        at_sp(lax.rem(sp + 2, nsp)),
        at_sp(lax.rem(sp + nsp - 2, nsp)),
    )
    partner = at_sp(sp + 1 - 2 * core)
    across = [{"tp": lax.rem(x + o, nx)} for o in range(1, nx)]
    greet([hop_to[0], hop_to[1], partner] + across)

    wo_rows = wo_ref.shape[0]

    def source(way, s):
        return lax.rem(z + nz - (s + 1), nz) if way == 0 else lax.rem(z + s + 1, nz)

    def piece(block, c):
        return kv.at[c // 2, block, pl.ds((c % 2) * half, half)]

    def own_piece(c):
        return (k_ref, v_ref)[c // 2].at[pl.ds((c % 2) * half, half)]

    def ring(way, s, c, block, src=None):
        return remote(
            piece(block, c) if src is None else src,
            piece(block, c),
            ring_send.at[way, s, c],
            ring_recv.at[way, s, c],
            hop_to[way],
        )

    def pair(way, s, c, block):
        return remote(
            piece(block, c),
            piece(block, c),
            pair_send.at[way, s, c],
            pair_recv.at[way, s, c],
            partner,
        )

    def own_pair(c, block):
        return remote(own_piece(c), piece(block, c), own_send.at[c], own_recv.at[c], partner)

    def aux_hop(way, s, block, src=None):
        return remote(
            aux_out.at[block] if src is None else src,
            aux_out.at[block],
            aux_send.at[way, s],
            aux_recv.at[way, s],
            hop_to[way],
        )

    def wo_copy(o, at):
        return remote(
            wo_ref,
            wo_out.at[pl.ds(at * wo_rows, wo_rows)],
            wo_send.at[o - 1],
            wo_recv.at[o - 1],
            across[o - 1],
        )

    for way in (0, 1):
        aux_hop(way, 0, z, aux_ref).start()
    for c in range(4):
        for way in (0, 1):
            ring(way, 0, c, sp, own_piece(c)).start()
        own_pair(c, sp).start()
    for o in range(1, nx):
        wo_copy(o, x).start()

    kv[0, sp] = k_ref[...]
    kv[1, sp] = v_ref[...]
    aux_out[z] = aux_ref[...]
    wo_out[pl.ds(x * wo_rows, wo_rows), :] = wo_ref[...]
    acc[...] = jnp.zeros_like(acc)
    behind[...] = jnp.zeros_like(behind)
    far[...] = jnp.zeros_like(far)

    tile = min(256, rows)
    above = lax.broadcasted_iota(jnp.int32, (KBLK, 2 * KBLK), 0)
    below = lax.broadcasted_iota(jnp.int32, (KBLK, 2 * KBLK), 1)
    sums = ((above > below) | (below >= KBLK)).astype(F32).astype(BF16)
    to_log2 = HEAD_DIM ** (-0.5) * LOG2E

    def visit(block, mode):
        @pl.loop(0, rows // tile)
        def _(t):
            here = pl.ds(pl.multiple_of(t * tile, tile), tile)
            q = q_ref[here, :]
            spent_after = (
                jnp.zeros((tile, KBLK), F32) if mode == "far" else behind[here, :]
            )
            total = jnp.zeros((tile, HEAD_DIM), F32)
            for b in reversed(range(rows // KBLK)):
                span = pl.ds(b * KBLK, KBLK)
                score = (
                    lax.dot_general(
                        q,
                        kv[0, block, span, :],
                        (((1,), (1,)), ((), ())),
                        preferred_element_type=F32,
                    )
                    * to_log2
                )
                soft = jnp.maximum(
                    score, jnp.log(1.0 + jnp.exp2(jnp.minimum(score, 64.0))) * LOG2E
                )
                if mode == "diagonal":
                    key_pos = b * KBLK + lax.broadcasted_iota(jnp.int32, (tile, KBLK), 1)
                    query_pos = t * tile + lax.broadcasted_iota(jnp.int32, (tile, KBLK), 0)
                    usable = key_pos < query_pos
                    spent = jnp.where(usable, soft, 0.0)
                else:
                    spent = soft
                added = jnp.dot(spent.astype(BF16), sums, preferred_element_type=F32)
                weight = jnp.exp2(((score - soft) - added[:, :KBLK]) - spent_after)
                if mode == "diagonal":
                    weight = jnp.where(usable, weight, 0.0)
                spent_after = spent_after + added[:, KBLK:]
                total = total + jnp.dot(
                    weight.astype(BF16), kv[1, block, span, :], preferred_element_type=F32
                )
            if mode == "far":
                far[here, :] = far[here, :] * jnp.exp2(-spent_after) + total
            else:
                acc[here, :] = acc[here, :] + total
                behind[here, :] = spent_after

    def work(s, c):
        near_chip = z - (s + 1)
        far_chip = z + s + 1 - nz
        if c < 2:

            @pl.when(near_chip >= 0)
            def _():
                visit(jnp.maximum(2 * near_chip + 1 - c, 0), "near")

        else:

            @pl.when(far_chip >= 0)
            def _():
                visit(jnp.maximum(2 * far_chip + c - 2, 0), "far")

    visit(sp, "diagonal")
    other = sp + 1 - 2 * core
    for c in range(4):
        own_pair(c, other).wait_recv()

    @pl.when(core == 1)
    def _():
        visit(other, "near")

    def of_pair(way, s):
        return 2 * source(way, s) + 1 - core

    @pl.loop(0, far_hop)
    def _(s):
        for way in (0, 1):
            aux_hop(way, s, source(way, s)).wait_recv()

            @pl.when((s < far_hop - 1) | (way == 0))
            def _():
                aux_hop(way, s + 1, source(way, s)).start()

        for c in range(4):
            for way in (0, 1):
                block = 2 * source(way, s) + core
                ring(way, s, c, block).wait_recv()
                if (c < 2) == (way == 0):
                    ring(way, s + 1, c, block).start()
                else:

                    @pl.when(s < far_hop - 1)
                    def _():
                        ring(way, s + 1, c, block).start()

                pair(way, s, c, block).start()

            @pl.when(s > 0)
            def _():
                if c == 0:
                    for way in (0, 1):
                        for c2 in range(4):
                            pair(way, s - 1, c2, of_pair(way, s - 1)).wait_recv()
                work(s - 1, c)

    last = far_hop - 1
    for way in (0, 1):
        for c2 in range(4):
            pair(way, last, c2, of_pair(way, last)).wait_recv()
    for c in range(4):
        work(last, c)
    aux_hop(0, far_hop, source(0, far_hop)).wait_recv()
    for c in range(4):
        way = c // 2
        block = 2 * source(way, far_hop) + core
        ring(way, far_hop, c, block).wait_recv()
        pair(way, far_hop, c, block).start()
    for c in range(4):
        way = c // 2
        pair(way, far_hop, c, of_pair(way, far_hop)).wait_recv()
    for c in range(2):
        work(far_hop, c)
    out_ref[...] = (acc[...] + far[...] * jnp.exp2(-behind[...])).astype(out_ref.dtype)

    for o in range(1, nx):
        wo_copy(o, lax.rem(x + nx - o, nx)).wait_recv()
        wo_copy(o, x).wait_send()
    for c in range(4):
        own_pair(c, sp).wait_send()

    @pl.loop(0, far_hop)
    def _(s):
        for way in (0, 1):
            aux_hop(way, s, z).wait_send()
            for c in range(4):
                ring(way, s, c, sp).wait_send()
                pair(way, s, c, sp).wait_send()

    aux_hop(0, far_hop, z).wait_send()
    for c in range(4):
        ring(c // 2, far_hop, c, sp).wait_send()
        pair(c // 2, far_hop, c, sp).wait_send()


def attention(nz, nx, q, k, v, wo, aux):
    rows, width = q.shape
    whole = pl.BlockSpec(memory_space=pltpu.VMEM)
    hops = nz // 2
    dma = pltpu.SemaphoreType.DMA
    flops = 6 * rows * rows * width * nz * 2
    return pl.pallas_call(
        functools.partial(attention_kernel, nz, nx),
        name="attention",
        out_shape=(
            jax.ShapeDtypeStruct((rows, width), BF16),
            jax.ShapeDtypeStruct((nx * wo.shape[0], wo.shape[1]), BF16),
            jax.ShapeDtypeStruct((nz, *aux.shape), F32),
        ),
        in_specs=[whole] * 5,
        out_specs=(whole, whole, whole),
        scratch_shapes=[
            pltpu.VMEM((2, 2 * nz, rows, width), BF16),
            pltpu.VMEM((rows, width), F32),
            pltpu.VMEM((rows, KBLK), F32),
            pltpu.VMEM((rows, width), F32),
            dma((2, hops, 4)),
            dma((2, hops, 4)),
            dma((2, hops, 4)),
            dma((2, hops, 4)),
            dma((4,)),
            dma((4,)),
            dma((2, hops)),
            dma((2, hops)),
            dma((nx - 1,)),
            dma((nx - 1,)),
        ],
        compiler_params=pltpu.CompilerParams(collective_id=0, has_side_effects=True),
        cost_estimate=pl.CostEstimate(flops=flops, bytes_accessed=1 << 20, transcendentals=0),
    )(q, k, v, wo, aux)


def slot_codes(aux, z, experts):
    width = aux.shape[1]
    picks = aux.shape[0] // 2
    number = (z * experts + lax.broadcasted_iota(jnp.int32, (experts, width), 0)).astype(F32)
    named = jnp.zeros((experts, width), F32)
    share = jnp.zeros((experts, width), F32)
    for k in range(picks):
        hit = aux[k : k + 1, :] == number
        named = named + jnp.where(hit, 1.0, 0.0)
        share = share + jnp.where(hit, aux[picks + k : picks + k + 1, :], 0.0)
    earlier = lax.broadcasted_iota(jnp.int32, (width, width), 0)
    later = lax.broadcasted_iota(jnp.int32, (width, width), 1)
    before = (earlier < later).astype(F32).astype(BF16)
    rank = jnp.dot(named.astype(BF16), before, preferred_element_type=F32)
    return jnp.where(named > 0.0, rank, -1000.0), share


def slot_matches(code, side):
    experts, width = code.shape
    slot = lax.broadcasted_iota(jnp.int32, (experts, 2 * SLOTS, width), 1).astype(F32)
    return (code[:, None, :] + float(side * SLOTS)) == slot


def norm(summed, gains, offset):
    average = jnp.mean(summed, axis=-1, keepdims=True)
    centred = summed - average
    spread = jnp.mean(centred * centred, axis=-1, keepdims=True)
    return centred * lax.rsqrt(spread + NORM_EPS) * gains + offset


def gated(gate_act, up_act):
    return (gate_act / (1.0 + jnp.exp(-gate_act)) * up_act).astype(BF16)


CHUNKS = 4


def group_peers(nx, core, x, z):
    me = core * nx + x
    peers = []
    for o in range(1, 2 * nx):
        i = lax.rem(me + o, 2 * nx)
        peers.append((i, {"sp": 2 * z + i // nx, "tp": lax.rem(i, nx)}))
    return me, peers


def dispatch_kernel(
    nz,
    nx,
    att_ref,
    wo_ref,
    res_ref,
    aux_ref,
    gain_ref,
    bias_ref,
    gate_hbm,
    up_hbm,
    down_hbm,
    sgate_hbm,
    sup_hbm,
    sdown_hbm,
    made_ref,
    base_ref,
    heads,
    rows_all,
    outgoing,
    slots,
    gate,
    up,
    down,
    sgate,
    sup,
    sdown,
    load_sem,
    head_send,
    head_recv,
    ring_send,
    ring_recv,
    slot_send,
    slot_recv,
):
    sp, z, core, x = place()
    nsp = 2 * nz
    tokens, width = res_ref.shape
    part = tokens // CHUNKS
    far_hop = nz // 2 - 1
    hop_to = (
        at_sp(lax.rem(sp + 2, nsp)),
        at_sp(lax.rem(sp + nsp - 2, nsp)),
    )
    me, peers = group_peers(nx, core, x, z)
    greet([hop_to[0], hop_to[1]] + [device for _, device in peers])

    def head_copy(o, to, at):
        return remote(
            att_ref.at[pl.ds(to * tokens, tokens)],
            heads.at[at],
            head_send.at[o - 1],
            head_recv.at[o - 1],
            {"tp": lax.rem(x + o, nx)},
        )

    for o in range(1, nx):
        head_copy(o, lax.rem(x + o, nx), x).start()

    loads = [
        pltpu.make_async_copy(src, dst, load_sem.at[n])
        for n, (src, dst) in enumerate(
            (
                (sgate_hbm, sgate),
                (sup_hbm, sup),
                (sdown_hbm, sdown),
                (gate_hbm, gate),
                (up_hbm, up),
                (down_hbm, down),
            )
        )
    ]
    for load in loads:
        load.start()

    heads[x] = att_ref[pl.ds(x * tokens, tokens), :]
    for o in range(1, nx):
        head_copy(o, x, lax.rem(x + nx - o, nx)).wait_recv()

    def source(way, s):
        return lax.rem(z + nz - (s + 1), nz) if way == 0 else lax.rem(z + s + 1, nz)

    def ring(way, s, c, block):
        piece = rows_all.at[block, pl.ds(c * part, part)]
        return remote(
            piece, piece, ring_send.at[way, s, c], ring_recv.at[way, s, c], hop_to[way]
        )

    by_token = jnp.concatenate([heads[i] for i in range(nx)], axis=1)
    mixed = jnp.dot(by_token, wo_ref[...], preferred_element_type=F32)
    normed = norm(
        res_ref[...].astype(F32) + mixed, gain_ref[...], bias_ref[...]
    ).astype(BF16)
    rows_all[z] = normed
    base_ref[...] = normed.astype(F32)

    for c in range(CHUNKS):
        for way in (0, 1):
            ring(way, 0, c, z).start()

    experts = 2 * nx

    def forward(s, block, way, c):
        ring(way, s, c, block).wait_recv()

    def chosen(block, side):
        code, _ = slot_codes(aux_ref[block], z, experts)
        picks = slot_matches(code, side)
        flat = jnp.where(picks, 1.0, 0.0).reshape(experts * 2 * SLOTS, tokens)
        return jnp.dot(flat.astype(BF16), rows_all[block], preferred_element_type=F32)

    def slot_copy(o, i, device, g, at):
        return remote(
            outgoing.at[i, g], slots.at[at, g], slot_send.at[o, g], slot_recv.at[o, g], device
        )

    def hand_out(first, second, g):
        found = chosen(first, 0) + chosen(second, 1)
        outgoing[:, g] = found.astype(BF16).reshape(experts, 2 * SLOTS, width)
        slots[me, g] = outgoing[me, g]
        for o, (i, device) in enumerate(peers):
            slot_copy(o, i, device, g, me).start()

    for load in loads[:3]:
        load.wait()
    own = rows_all[z]
    shared_hidden = gated(
        jnp.dot(own, sgate[...], preferred_element_type=F32),
        jnp.dot(own, sup[...], preferred_element_type=F32),
    )
    base_ref[...] += jnp.dot(shared_hidden, sdown[...], preferred_element_type=F32)

    @pl.loop(0, far_hop)
    def _(s):
        for c in range(CHUNKS):
            for way in (0, 1):
                block = source(way, s)
                ring(way, s, c, block).wait_recv()
                if (c < CHUNKS // 2) == (way == 0):
                    ring(way, s + 1, c, block).start()
                else:

                    @pl.when(s < far_hop - 1)
                    def _():
                        ring(way, s + 1, c, block).start()

        hand_out(source(0, s), source(1, s), s)

    for c in range(CHUNKS):
        way = 0 if c < CHUNKS // 2 else 1
        ring(way, far_hop, c, source(way, far_hop)).wait_recv()
    hand_out(source(0, far_hop), z, far_hop)

    for load in loads[3:]:
        load.wait()

    @pl.loop(0, nz // 2)
    def _(g):
        for o, (i, device) in enumerate(peers):
            slot_copy(o, i, device, g, i).wait_recv()

    together = 2
    lines = together * (nz // 2) * 2 * SLOTS

    @pl.loop(0, experts // together)
    def _(n):
        at = pl.ds(n * together, together)
        given = slots[at].reshape(lines, width)
        hidden = gated(
            jnp.dot(given, gate[0], preferred_element_type=F32),
            jnp.dot(given, up[0], preferred_element_type=F32),
        )
        made = jnp.dot(hidden, down[0], preferred_element_type=F32)
        made_ref[at] = made.astype(BF16).reshape(together, nz // 2, 2 * SLOTS, width)

    for o in range(1, nx):
        head_copy(o, x, x).wait_send()

    @pl.loop(0, far_hop)
    def _(s):
        for way in (0, 1):
            for c in range(CHUNKS):
                ring(way, s, c, z).wait_send()

    for c in range(CHUNKS):
        ring(0 if c < CHUNKS // 2 else 1, far_hop, c, z).wait_send()

    @pl.loop(0, nz // 2)
    def _(g):
        for o, (i, device) in enumerate(peers):
            slot_copy(o, i, device, g, i).wait_send()


def dispatch(nz, nx, att, wo, res, aux, gain, bias, weights, shared):
    tokens, width = res.shape
    groups = nz // 2
    experts = 2 * nx
    whole = pl.BlockSpec(memory_space=pltpu.VMEM)
    anywhere = pl.BlockSpec(memory_space=pl.ANY)
    dma = pltpu.SemaphoreType.DMA
    slot_shape = (experts, groups, 2 * SLOTS, width)
    return pl.pallas_call(
        functools.partial(dispatch_kernel, nz, nx),
        name="dispatch",
        out_shape=(
            jax.ShapeDtypeStruct(slot_shape, BF16),
            jax.ShapeDtypeStruct((tokens, width), F32),
        ),
        in_specs=[whole] * 6 + [anywhere] * 6,
        out_specs=(whole, whole),
        scratch_shapes=[
            pltpu.VMEM((nx, tokens, HEAD_DIM), BF16),
            pltpu.VMEM((nz, tokens, width), BF16),
            pltpu.VMEM(slot_shape, BF16),
            pltpu.VMEM(slot_shape, BF16),
            *[pltpu.VMEM(w.shape, BF16) for w in (*weights, *shared)],
            dma((6,)),
            dma((nx - 1,)),
            dma((nx - 1,)),
            dma((2, groups, CHUNKS)),
            dma((2, groups, CHUNKS)),
            dma((experts - 1, groups)),
            dma((experts - 1, groups)),
        ],
        compiler_params=pltpu.CompilerParams(collective_id=1, has_side_effects=True),
        cost_estimate=pl.CostEstimate(flops=1 << 33, bytes_accessed=1 << 24, transcendentals=0),
    )(att, wo, res, aux, gain, bias, *weights, *shared)


def collect_kernel(
    nz,
    nx,
    made_ref,
    base_ref,
    aux_ref,
    gain_ref,
    bias_ref,
    out_ref,
    back,
    held,
    sums,
    back_send,
    back_recv,
    ring_send,
    ring_recv,
):
    sp, z, core, x = place()
    nsp = 2 * nz
    tokens, width = base_ref.shape
    part = tokens // CHUNKS
    hops = nz // 2
    hop_to = (
        at_sp(lax.rem(sp + 2, nsp)),
        at_sp(lax.rem(sp + nsp - 2, nsp)),
    )
    me, peers = group_peers(nx, core, x, z)
    greet([hop_to[0], hop_to[1]] + [device for _, device in peers])
    experts = 2 * nx
    last = hops - 1

    def back_copy(o, i, device, g, at):
        return remote(
            made_ref.at[i, g], back.at[at, g], back_send.at[o, g], back_recv.at[o, g], device
        )

    @pl.loop(0, hops)
    def _(n):
        for o, (i, device) in enumerate(peers):
            back_copy(o, i, device, last - n, me).start()

    back[me] = made_ref[me]

    def arrived(g):
        for o, (i, device) in enumerate(peers):
            back_copy(o, i, device, g, i).wait_recv()

    def weighed(token_chip, side, g):
        code, share = slot_codes(aux_ref[token_chip], z, experts)
        picks = slot_matches(code, side)
        flat = jnp.where(picks, share[:, None, :], 0.0).reshape(experts * 2 * SLOTS, tokens)
        lines = back[:, g].reshape(experts * 2 * SLOTS, width)
        return jnp.dot(flat.T.astype(BF16), lines, preferred_element_type=F32)

    def ring(way, s, c):
        at = pl.ds(c * part, part)
        return remote(
            sums.at[way, s, at],
            held.at[way, s, at],
            ring_send.at[way, s, c],
            ring_recv.at[way, s, c],
            hop_to[way],
        )

    def first_half(c):
        return c < CHUNKS // 2

    def rows_of(c):
        return slice(c * part, (c + 1) * part)

    arrived(last)
    opposite = lax.rem(z + hops, nz)
    far = weighed(opposite, 0, last).astype(BF16)
    for c in range(CHUNKS):
        way = 0 if first_half(c) else 1
        sums[way, 0, rows_of(c), :] = far[rows_of(c), :]
        ring(way, 0, c).start()

    def step(s, received):
        g = last - s
        arrived(g)
        own = (
            weighed(lax.rem(z + hops - s, nz), 1, g),
            weighed(lax.rem(z + nz - hops + s, nz), 0, g),
        )
        for c in range(CHUNKS):
            for way in (0, 1):
                summed = own[way][rows_of(c), :]
                if received(way, c):
                    ring(way, s - 1, c).wait_recv()
                    summed = summed + held[way, s - 1, rows_of(c), :].astype(F32)
                sums[way, s, rows_of(c), :] = summed.astype(BF16)
                ring(way, s, c).start()

    step(1, lambda way, c: first_half(c) == (way == 0))

    @pl.loop(2, hops)
    def _(s):
        step(s, lambda way, c: True)

    base = base_ref[...] + weighed(z, 1, last)
    for c in range(CHUNKS):
        at = rows_of(c)
        for way in (0, 1):
            ring(way, last, c).wait_recv()
        summed = (
            base[at, :]
            + held[0, last, at, :].astype(F32)
            + held[1, last, at, :].astype(F32)
        )
        out_ref[at, :] = norm(summed, gain_ref[...], bias_ref[...]).astype(out_ref.dtype)

    for c in range(CHUNKS):
        ring(0 if first_half(c) else 1, 0, c).wait_send()

    @pl.loop(1, hops)
    def _(s):
        for way in (0, 1):
            for c in range(CHUNKS):
                ring(way, s, c).wait_send()

    @pl.loop(0, hops)
    def _(g):
        for o, (i, device) in enumerate(peers):
            back_copy(o, i, device, g, i).wait_send()


def collect(nz, nx, made, base, aux, gain, bias):
    tokens, width = base.shape
    hops = nz // 2
    experts = 2 * nx
    whole = pl.BlockSpec(memory_space=pltpu.VMEM)
    dma = pltpu.SemaphoreType.DMA
    return pl.pallas_call(
        functools.partial(collect_kernel, nz, nx),
        name="collect",
        out_shape=jax.ShapeDtypeStruct((tokens, width), BF16),
        in_specs=[whole] * 5,
        out_specs=whole,
        scratch_shapes=[
            pltpu.VMEM(made.shape, BF16),
            pltpu.VMEM((2, hops, tokens, width), BF16),
            pltpu.VMEM((2, hops, tokens, width), BF16),
            dma((experts - 1, hops)),
            dma((experts - 1, hops)),
            dma((2, hops, CHUNKS)),
            dma((2, hops, CHUNKS)),
        ],
        compiler_params=pltpu.CompilerParams(collective_id=2, has_side_effects=True),
        cost_estimate=pl.CostEstimate(flops=1 << 32, bytes_accessed=1 << 24, transcendentals=0),
    )(made, base, aux, gain, bias)


def local(
    query_rows,
    key_rows,
    value_rows,
    residual,
    output_weight,
    first_gain,
    first_bias,
    expert_ids,
    expert_share,
    gate_weight,
    up_weight,
    down_weight,
    shared_gate,
    shared_up,
    shared_down,
    second_gain,
    second_bias,
):
    nz = lax.axis_size("sp") // 2
    nx = lax.axis_size("tp")
    aux = jnp.concatenate([expert_ids.T.astype(F32), expert_share.T], axis=0)
    attended, wo, aux_all = attention(
        nz, nx, query_rows, key_rows, value_rows, output_weight, aux
    )
    made, base = dispatch(
        nz,
        nx,
        attended,
        wo,
        residual,
        aux_all,
        first_gain[None, :],
        first_bias[None, :],
        (gate_weight, up_weight, down_weight),
        (shared_gate, shared_up, shared_down),
    )
    return collect(nz, nx, made, base, aux_all, second_gain[None, :], second_bias[None, :])


def solution(mesh):
    return jax.shard_map(
        local,
        mesh=mesh,
        in_specs=(
            P(("grp", "sp"), "tp"),
            P(("grp", "sp"), "tp"),
            P(("grp", "sp"), "tp"),
            P(("grp", "sp", "tp"), None),
            P("tp", None),
            P(),
            P(),
            P(("grp", "sp", "tp"), None),
            P(("grp", "sp", "tp"), None),
            P(("sp", "tp"), None, None),
            P(("sp", "tp"), None, None),
            P(("sp", "tp"), None, None),
            P(),
            P(),
            P(),
            P(),
            P(),
        ),
        out_specs=P(("grp", "sp", "tp"), None),
        check_vma=False,
    )
```

time: 938 us -> 312 us (0.33)
  blocking collectives: 525 us -> 0 us
  Pallas kernels: 0 us -> 307 us
  waiting for transfers between devices: 273 us -> 0 us
  local copies, waits for them, and re-layouts: 58.8 us -> 1.88 us
  matrix products: 31.8 us -> 0 us
  starting transfers between devices: 20.3 us -> 0 us
  between operations: 13.6 us -> 0.03 us
    all_to_all x1 -> x0, blocking collectives: 525 us -> none  [local(): lax.all_to_all(outgoing, ('sp', 'tp'), split_axis=0, concat_axis=0, tiled...]
    pallas_call x0 -> x3, Pallas kernels: none -> 307 us  [the longest x1 123 us: dispatch(): pl.pallas_call(functools.partial(dispatch_kernel, nz, nx), name='dispatch...]
    all_to_all x3 -> x0, waiting for transfers between devices: 189 us -> none  [the longest x1 184 us: local(): lax.all_to_all(results, ('sp', 'tp'), split_axis=0, concat_axis=0, tiled=...]
    all_gather x1 -> x0, waiting for transfers between devices: 84.1 us -> none  [in_one_piece(): lax.all_gather(both, axis, axis=dim, tiled=True)]
    dot_general x10 -> x0, matrix products: 31.8 us -> none  [the longest x1 7.81 us: local(): jnp.dot(hidden, down_weight[0], preferred_element_type=jnp.float32)]
    reshape x7 -> x0, local copies, waits for them, and re-layouts: 30.9 us -> none  [the longest x1 6.34 us: local(): flat_rows = slot_rows.reshape(-1, width)]
    all_to_all x3 -> x0, starting transfers between devices: 20.3 us -> none  [the longest x1 11.1 us: local(): lax.all_to_all(results, ('sp', 'tp'), split_axis=0, concat_axis=0, tiled=...]
    gather x2 -> x0, local copies, waits for them, and re-layouts: 11.7 us -> none  [local(): jnp.take(flat_back, slot_ids, axis=0).reshape(tokens_here, top_count, width)]
  transfers between devices with their start and end apart: 4 -> 0, of which waited for: 3 -> 0; matrix products, arithmetic and copies ran while one was open for 4% -> 0% of each run, Pallas kernels for 0% -> 0%
where the time goes in v1:
time: 312 us; the launch traced here: 311 us
  Pallas kernels  307 us (98%)
    pallas_call x1, Pallas kernels, dispatch(): pl.pallas_call(functools.partial(dispatch_kernel, nz, nx), name='dispatch...  123 us
    pallas_call x1, Pallas kernels, collect(): pl.pallas_call(functools.partial(collect_kernel, nz, nx), name='collect',...  103 us
    pallas_call x1, Pallas kernels, attention(): pl.pallas_call(functools.partial(attention_kernel, nz, nx), name='attenti...  81.3 us

profile of v1, /device:TPU:33, one launch (start us, length us, event | category | flops | bytes accessed | tf_op | source)
XLA Modules:
  0.0 310.9 jit_solution(5003344471313057785)
XLA Ops:
  0.0 0.7 convert_bitcast_fusion
  0.7 1.3 pad_maximum_fusion.aux_ref
  2.0 81.3 %attention.1 = (bf16[512,128]{1,0:T(8,128)(2,1)}, bf16[512,2048]{1,0:T(8,128)(2,1)}, f32[16,8,128]{2,1,0:T(8,128)}) custom-call(bf16[512,128]{1,0:T(8,128)(2,1)} %q_ref.1, bf16[512,128]{1,0:T(8,128)(2,1)} %k_ref.1, bf16[512,128]{1,0:T(8,128)(2,1)} %v_ref.1, bf16[128,2048]{1,0:T(8,128)(2,1)} %wo_ref.1, f32[8,128]{1,0:T(8,128)} %pad_maximum_fusion.aux_ref), custom_call_target="tpu_custom_call" | custom-call | flops 6442450944 | bytes 1048576 | tf_op jit(solution)/shard_map/attention/pallas_call | solution.py:306
  83.2 122.9 %dispatch.1 = (bf16[8,8,16,2048]{3,2,1,0:T(8,128)(2,1)}, f32[128,2048]{1,0:T(8,128)}) custom-call(bf16[512,128]{1,0:T(8,128)(2,1)} %get-tuple-element.10.att_ref, bf16[512,2048]{1,0:T(8,128)(2,1)} %get-tuple-element.11.wo_ref, bf16[128,2048]{1,0:T(8,128)(2,1)} %res_ref.1, f32[16,8,128]{2,1,0:T(8,128)} %get-tuple-element.12.aux_ref, f32[1,2048]{1,0:T(1,128)} %bitcast.8, ...), custom_call_target="tpu_custom_call" | custom-call | flops 8589934592 | bytes 16777216 | tf_op jit(solution)/shard_map/dispatch/pallas_call | solution.py:584
  206.2 102.8 %collect.1 = bf16[128,2048]{1,0:T(8,128)(2,1)} custom-call(bf16[8,8,16,2048]{3,2,1,0:T(8,128)(2,1)} %get-tuple-element.13.made_ref, f32[128,2048]{1,0:T(8,128)} %get-tuple-element.14.base_ref, f32[16,8,128]{2,1,0:T(8,128)} %get-tuple-element.12.aux_ref, f32[1,2048]{1,0:T(1,128)} %bitcast.10, f32[1,2048]{1,0:T(1,128)} %bitcast.11), custom_call_target="tpu_custom_call" | custom-call | flops 4294967296 | bytes 16777216 | tf_op jit(solution)/shard_map/collect/pallas_call | solution.py:745
  309.0 1.9 copy.19

commit v2 on v0

v2 whole, which is shorter than its diff:
```python
import functools

import jax
import jax.numpy as jnp
from jax import lax
from jax.experimental import pallas as pl
from jax.experimental.pallas import tpu as pltpu
from jax.sharding import PartitionSpec as P

HEAD_DIM = 128
KBLK = 128
NORM_EPS = 1e-05
LOG2E = 1.4426950408889634
MESH = pl.DeviceIdType.MESH
SLOTS = 8
USED = 6
BF16 = jnp.bfloat16
F32 = jnp.float32


def at_sp(sp):
    return {"sp": sp}


def place():
    sp = lax.axis_index("sp")
    return sp, sp // 2, sp % 2, lax.axis_index("tp")


def greet(devices):
    barrier = pltpu.get_barrier_semaphore()
    for device in devices:
        pl.semaphore_signal(barrier, inc=1, device_id=device, device_id_type=MESH)
    pl.semaphore_wait(barrier, len(devices))


def remote(src, dst, send_sem, recv_sem, device):
    return pltpu.make_async_remote_copy(
        src_ref=src,
        dst_ref=dst,
        send_sem=send_sem,
        recv_sem=recv_sem,
        device_id=device,
        device_id_type=MESH,
    )


def slot_codes(aux, z, experts):
    width = aux.shape[1]
    picks = aux.shape[0] // 2
    number = (z * experts + lax.broadcasted_iota(jnp.int32, (experts, width), 0)).astype(F32)
    named = jnp.zeros((experts, width), F32)
    share = jnp.zeros((experts, width), F32)
    for k in range(picks):
        hit = aux[k : k + 1, :] == number
        named = named + jnp.where(hit, 1.0, 0.0)
        share = share + jnp.where(hit, aux[picks + k : picks + k + 1, :], 0.0)
    earlier = lax.broadcasted_iota(jnp.int32, (width, width), 0)
    later = lax.broadcasted_iota(jnp.int32, (width, width), 1)
    before = (earlier < later).astype(F32).astype(BF16)
    rank = jnp.dot(named.astype(BF16), before, preferred_element_type=F32)
    return jnp.where(named > 0.0, rank, -1000.0), share


def slot_matches(code, side):
    experts, width = code.shape
    slot = lax.broadcasted_iota(jnp.int32, (experts, 2 * SLOTS, width), 1).astype(F32)
    return (code[:, None, :] + float(side * SLOTS)) == slot


def norm(summed, gains, offset):
    average = jnp.mean(summed, axis=-1, keepdims=True)
    centred = summed - average
    spread = jnp.mean(centred * centred, axis=-1, keepdims=True)
    return centred * lax.rsqrt(spread + NORM_EPS) * gains + offset


def gated(gate_act, up_act):
    return (gate_act / (1.0 + jnp.exp(-gate_act)) * up_act).astype(BF16)


CHUNKS = 4


def group_peers(nx, core, x, z):
    me = core * nx + x
    peers = []
    for o in range(1, 2 * nx):
        i = lax.rem(me + o, 2 * nx)
        peers.append((i, {"sp": 2 * z + i // nx, "tp": lax.rem(i, nx)}))
    return me, peers


class Names:
    pass


def layer_kernel(nz, nx, *refs):
    sp, z, core, x = place()
    nsp = 2 * nz
    r = Names()
    for name, ref in zip(REFS, refs, strict=True):
        setattr(r, name, ref)
    hop_to = (at_sp(lax.rem(sp + 2, nsp)), at_sp(lax.rem(sp + nsp - 2, nsp)))
    partner = at_sp(sp + 1 - 2 * core)
    across = [{"tp": lax.rem(x + o, nx)} for o in range(1, nx)]
    me, peers = group_peers(nx, core, x, z)

    def shift(way, by):
        return lax.rem(z + by, nz) if way == 0 else lax.rem(z + nz - by, nz)

    def member(chip, i):
        return {"sp": 2 * chip + i // nx, "tp": i % nx}

    r.raw_in[...] = jnp.zeros_like(r.raw_in)
    greet(
        [device for _, device in peers]
        + [
            member(shift(way, by), i)
            for by in (1, 2)
            for way in (0, 1)
            for i in range(2 * nx)
        ]
    )

    hops = nz // 2
    last = hops - 1
    experts = 2 * nx
    tokens, width = r.res.shape
    rows = r.q.shape[0]

    loads = [
        pltpu.make_async_copy(src, dst, r.load_sem.at[n])
        for n, (src, dst) in enumerate(
            (
                (r.sgate_hbm, r.sgate),
                (r.sup_hbm, r.sup),
                (r.sdown_hbm, r.sdown),
                (r.gate_hbm, r.gate),
                (r.up_hbm, r.up),
                (r.down_hbm, r.down),
            )
        )
    ]

    def source(way, s):
        return lax.rem(z + nz - (s + 1), nz) if way == 0 else lax.rem(z + s + 1, nz)


    half = rows // 2
    wo_rows = r.wo.shape[0]

    def piece(block, c):
        return r.kv.at[c // 2, block, pl.ds((c % 2) * half, half)]

    def own_piece(c):
        return (r.k, r.v)[c // 2].at[pl.ds((c % 2) * half, half)]

    def ring(way, s, c, block, src=None):
        return remote(
            piece(block, c) if src is None else src,
            piece(block, c),
            r.kv_send.at[way, s, c],
            r.kv_recv.at[way, s, c],
            hop_to[way],
        )

    def pair(way, s, c, block):
        return remote(
            piece(block, c),
            piece(block, c),
            r.pair_send.at[way, s, c],
            r.pair_recv.at[way, s, c],
            partner,
        )

    def own_pair(c, block):
        return remote(own_piece(c), piece(block, c), r.own_send.at[c], r.own_recv.at[c], partner)

    def aux_hop(way, s, block, src=None):
        return remote(
            r.aux_all.at[block] if src is None else src,
            r.aux_all.at[block],
            r.aux_send.at[way, s],
            r.aux_recv.at[way, s],
            hop_to[way],
        )

    def wo_copy(o, at):
        return remote(
            r.wo,
            r.wo_all.at[pl.ds(at * wo_rows, wo_rows)],
            r.wo_send.at[o - 1],
            r.wo_recv.at[o - 1],
            across[o - 1],
        )

    for way in (0, 1):
        aux_hop(way, 0, z, r.aux).start()
    for c in range(4):
        for way in (0, 1):
            ring(way, 0, c, sp, own_piece(c)).start()
        own_pair(c, sp).start()
    for o in range(1, nx):
        wo_copy(o, x).start()
    for load in loads:
        load.start()

    r.kv[0, sp] = r.k[...]
    r.kv[1, sp] = r.v[...]
    r.aux_all[z] = r.aux[...]
    r.wo_all[pl.ds(x * wo_rows, wo_rows), :] = r.wo[...]
    r.acc[...] = jnp.zeros_like(r.acc)
    r.behind[...] = jnp.zeros_like(r.behind)
    r.far[...] = jnp.zeros_like(r.far)

    tile = min(256, rows)
    above = lax.broadcasted_iota(jnp.int32, (KBLK, 2 * KBLK), 0)
    below = lax.broadcasted_iota(jnp.int32, (KBLK, 2 * KBLK), 1)
    sums = ((above > below) | (below >= KBLK)).astype(F32).astype(BF16)
    to_log2 = HEAD_DIM ** (-0.5) * LOG2E

    def visit(block, mode):
        @pl.loop(0, rows // tile)
        def _(t):
            here = pl.ds(pl.multiple_of(t * tile, tile), tile)
            q = r.q[here, :]
            spent_after = (
                jnp.zeros((tile, KBLK), F32) if mode == "far" else r.behind[here, :]
            )
            total = jnp.zeros((tile, HEAD_DIM), F32)
            for b in reversed(range(rows // KBLK)):
                span = pl.ds(b * KBLK, KBLK)
                score = (
                    lax.dot_general(
                        q,
                        r.kv[0, block, span, :],
                        (((1,), (1,)), ((), ())),
                        preferred_element_type=F32,
                    )
                    * to_log2
                )
                soft = jnp.maximum(
                    score, jnp.log(1.0 + jnp.exp2(jnp.minimum(score, 64.0))) * LOG2E
                )
                if mode == "diagonal":
                    key_pos = b * KBLK + lax.broadcasted_iota(jnp.int32, (tile, KBLK), 1)
                    query_pos = t * tile + lax.broadcasted_iota(jnp.int32, (tile, KBLK), 0)
                    usable = key_pos < query_pos
                    spent = jnp.where(usable, soft, 0.0)
                else:
                    spent = soft
                added = jnp.dot(spent.astype(BF16), sums, preferred_element_type=F32)
                weight = jnp.exp2(((score - soft) - added[:, :KBLK]) - spent_after)
                if mode == "diagonal":
                    weight = jnp.where(usable, weight, 0.0)
                spent_after = spent_after + added[:, KBLK:]
                total = total + jnp.dot(
                    weight.astype(BF16), r.kv[1, block, span, :], preferred_element_type=F32
                )
            if mode == "far":
                r.far[here, :] = r.far[here, :] * jnp.exp2(-spent_after) + total
            else:
                r.acc[here, :] = r.acc[here, :] + total
                r.behind[here, :] = spent_after

    def work(s, c):
        near_chip = z - (s + 1)
        far_chip = z + s + 1 - nz
        if c < 2:

            @pl.when(near_chip >= 0)
            def _():
                visit(jnp.maximum(2 * near_chip + 1 - c, 0), "near")

        else:

            @pl.when(far_chip >= 0)
            def _():
                visit(jnp.maximum(2 * far_chip + c - 2, 0), "far")

    def of_pair(way, s):
        return 2 * source(way, s) + 1 - core

    visit(sp, "diagonal")
    other = sp + 1 - 2 * core
    for c in range(4):
        own_pair(c, other).wait_recv()

    @pl.when(core == 1)
    def _():
        visit(other, "near")

    @pl.loop(0, last)
    def _(s):
        for way in (0, 1):
            aux_hop(way, s, source(way, s)).wait_recv()

            @pl.when((s < last - 1) | (way == 0))
            def _():
                aux_hop(way, s + 1, source(way, s)).start()

        for c in range(4):
            for way in (0, 1):
                block = 2 * source(way, s) + core
                ring(way, s, c, block).wait_recv()
                if (c < 2) == (way == 0):
                    ring(way, s + 1, c, block).start()
                else:

                    @pl.when(s < last - 1)
                    def _():
                        ring(way, s + 1, c, block).start()

                pair(way, s, c, block).start()

            @pl.when(s > 0)
            def _():
                if c == 0:
                    for way in (0, 1):
                        for c2 in range(4):
                            pair(way, s - 1, c2, of_pair(way, s - 1)).wait_recv()
                work(s - 1, c)

    for way in (0, 1):
        for c2 in range(4):
            pair(way, last - 1, c2, of_pair(way, last - 1)).wait_recv()
    for c in range(4):
        work(last - 1, c)
    aux_hop(0, last, source(0, last)).wait_recv()
    for c in range(4):
        way = c // 2
        block = 2 * source(way, last) + core
        ring(way, last, c, block).wait_recv()
        pair(way, last, c, block).start()
    for c in range(4):
        way = c // 2
        pair(way, last, c, of_pair(way, last)).wait_recv()
    for c in range(2):
        work(last, c)
    r.att[...] = (r.acc[...] + r.far[...] * jnp.exp2(-r.behind[...])).astype(BF16)


    def head_copy(o, to, at):
        return remote(
            r.att.at[pl.ds(to * tokens, tokens)],
            r.heads.at[at],
            r.head_send.at[o - 1],
            r.head_recv.at[o - 1],
            across[o - 1],
        )

    for o in range(1, nx):
        head_copy(o, lax.rem(x + o, nx), x).start()
    r.heads[x] = r.att[pl.ds(x * tokens, tokens), :]
    for o in range(1, nx):
        wo_copy(o, lax.rem(x + nx - o, nx)).wait_recv()
    for o in range(1, nx):
        head_copy(o, x, lax.rem(x + nx - o, nx)).wait_recv()
    by_token = jnp.concatenate([r.heads[i] for i in range(nx)], axis=1)
    mixed = jnp.dot(by_token, r.wo_all[...], preferred_element_type=F32)
    normed = norm(r.res[...].astype(F32) + mixed, r.gain1[...], r.bias1[...]).astype(BF16)
    r.rows_all[z] = normed


    part = tokens // CHUNKS

    def row_ring(way, s, c, block):
        at = r.rows_all.at[block, pl.ds(c * part, part)]
        return remote(at, at, r.row_send.at[way, s, c], r.row_recv.at[way, s, c], hop_to[way])

    for c in range(CHUNKS):
        for way in (0, 1):
            row_ring(way, 0, c, z).start()
    r.base[...] = r.rows_all[z].astype(F32)

    def chosen(block, side):
        code, _ = slot_codes(r.aux_all[block], z, experts)
        flat = jnp.where(slot_matches(code, side), 1.0, 0.0)
        flat = flat.reshape(experts * 2 * SLOTS, tokens).astype(BF16)
        return jnp.dot(flat, r.rows_all[block], preferred_element_type=F32)

    def outgoing_slot(g):
        return lax.rem(g, 2) if not isinstance(g, int) or g < last else 2

    def slot_copy(o, i, device, g, at, side=None):
        lines = pl.ds(0, 2 * SLOTS) if side is None else pl.ds(side * SLOTS, SLOTS)
        sem = g if side is None else last + side
        return remote(
            r.outgoing.at[i, outgoing_slot(g), lines],
            r.slots.at[at, g, lines],
            r.slot_send.at[o, sem],
            r.slot_recv.at[o, sem],
            device,
        )

    def send_slots(g):
        r.slots[me, g] = r.outgoing[me, outgoing_slot(g)]
        for o, (i, device) in enumerate(peers):
            slot_copy(o, i, device, g, me).start()

    def send_side(found, side):
        lines = slice(side * SLOTS, (side + 1) * SLOTS)
        found = found.astype(BF16).reshape(experts, 2 * SLOTS, width)
        r.outgoing[:, 2, lines] = found[:, lines]
        r.slots[me, last, lines] = r.outgoing[me, 2, lines]
        for o, (i, device) in enumerate(peers):
            slot_copy(o, i, device, last, me, side).start()

    def slots_sent(g):
        for o, (i, device) in enumerate(peers):
            slot_copy(o, i, device, g, i).wait_send()

    def fill(found, g):
        r.outgoing[:, outgoing_slot(g)] = found.astype(BF16).reshape(
            experts, 2 * SLOTS, width
        )
        send_slots(g)

    def back_copy(o, i, device, g, at, side=None):
        lines = pl.ds(0, 2 * SLOTS) if side is None else pl.ds(side * SLOTS, SLOTS)
        return remote(
            r.slots.at[i, g, lines],
            r.back.at[at, g, lines],
            r.back_send.at[o, g],
            r.back_recv.at[o, g],
            device,
        )

    def give_back(g, side=None):
        lines = slice(0, 2 * SLOTS) if side is None else slice(side * SLOTS, (side + 1) * SLOTS)
        r.back[me, g, lines] = r.slots[me, g, lines]
        for o, (i, device) in enumerate(peers):
            back_copy(o, i, device, g, me, side).start()

    def produce(g):
        given = r.slots[:, g].reshape(experts * 2 * SLOTS, width)
        hidden = gated(
            jnp.dot(given, r.gate[0], preferred_element_type=F32),
            jnp.dot(given, r.up[0], preferred_element_type=F32),
        )
        made = jnp.dot(hidden, r.down[0], preferred_element_type=F32)
        r.slots[:, g] = made.astype(BF16).reshape(experts, 2 * SLOTS, width)

    def serve(g):
        for o, (i, device) in enumerate(peers):
            slot_copy(o, i, device, g, i).wait_recv()
        produce(g)


    taken = pl.ds(0, USED)

    def far_send(way, n):
        chip = shift(way, 1) if n < experts else shift(way, 2)
        i = n if n < experts else way * nx + n - experts
        lines = pl.ds(way * SLOTS if n < experts else 0, USED)
        row = way if n < experts else 2
        return remote(
            r.far_out.at[way, n, taken],
            r.slots.at[me, last - 1 if n < experts else last, lines],
            r.far_send.at[way, n],
            r.far_recv.at[row, me],
            member(chip, i),
        )

    def far_arrival(row, i):
        side = row if row < 2 else 0
        here = r.slots.at[i, last - 1 if row < 2 else last, pl.ds(side * SLOTS, USED)]
        return remote(
            r.far_out.at[0, 0, taken], here, r.far_send.at[0, 0], r.far_recv.at[row, i], hop_to[0]
        )

    def far_return(row, i):
        way = row if row < 2 else core
        if row < 2:
            chip, n = shift(1 - row, 1), me
        else:
            chip, n = lax.rem(z + nz - 2 + 4 * core, nz), experts + x
        side = row if row < 2 else 0
        return remote(
            r.slots.at[i, last - 1 if row < 2 else last, pl.ds(side * SLOTS, USED)],
            r.raw_in.at[way, n, taken],
            r.raw_send.at[row, i],
            r.raw_recv.at[way, n],
            member(chip, i),
        )

    def raw_arrival(way, n):
        return remote(
            r.far_out.at[0, 0, taken],
            r.raw_in.at[way, n, taken],
            r.far_send.at[0, 0],
            r.raw_recv.at[way, n],
            hop_to[0],
        )

    def far_codes(way):
        aux = r.aux_all[source(way, last - 2)]
        code_one, share_one = slot_codes(aux, shift(way, 1), experts)
        code_two, share_two = slot_codes(aux, shift(way, 2), experts)
        part_two = slice(way * nx, (way + 1) * nx)
        code = jnp.concatenate([code_one, code_two[part_two]], axis=0)
        share = jnp.concatenate([share_one, share_two[part_two]], axis=0)
        slot = lax.broadcasted_iota(jnp.int32, (experts + nx, SLOTS, tokens), 1).astype(F32)
        return code[:, None, :] == slot, share[:, None, :]

    many = (experts + nx) * SLOTS

    def pass_on(way):
        picks, _ = far_codes(way)
        flat = jnp.where(picks, 1.0, 0.0).reshape(many, tokens).astype(BF16)
        found = jnp.dot(flat, r.rows_all[source(way, last - 2)], preferred_element_type=F32)
        r.far_out[way] = found.astype(BF16).reshape(experts + nx, SLOTS, width)
        for n in reversed(range(experts + nx)):
            far_send(way, n).start()

    for load in loads[:3]:
        load.wait()
    own = r.rows_all[z]
    shared_hidden = gated(
        jnp.dot(own, r.sgate[...], preferred_element_type=F32),
        jnp.dot(own, r.sup[...], preferred_element_type=F32),
    )
    r.base[...] += jnp.dot(shared_hidden, r.sdown[...], preferred_element_type=F32)
    send_side(chosen(z, 1), 1)
    for load in loads[3:]:
        load.wait()

    @pl.loop(0, last - 1)
    def _(s):
        for c in range(CHUNKS):
            for way in (0, 1):
                block = source(way, s)
                row_ring(way, s, c, block).wait_recv()

                @pl.when(s < last - 2)
                def _():
                    row_ring(way, s + 1, c, block).start()

        @pl.when(s == last - 2)
        def _():
            for way in (0, 1):
                pass_on(way)

        @pl.when(s > 1)
        def _():
            slots_sent(s - 2)

        fill(chosen(source(0, s), 0) + chosen(source(1, s), 1), s)

        @pl.when(s > 0)
        def _():
            serve(s - 1)

    serve(last - 2)
    for o, (i, device) in enumerate(peers):
        slot_copy(o, i, device, last, i, 1).wait_recv()
    for i in range(experts):
        far_arrival(2, i).wait_recv()
    produce(last)
    for i in range(experts):
        far_return(2, i).start()
    for row in (0, 1):
        for i in range(experts):
            far_arrival(row, i).wait_recv()
    produce(last - 1)
    for row in (0, 1):
        for i in range(experts):
            far_return(row, i).start()
    for g in (last - 2, last - 3, last - 4):
        give_back(g)
    give_back(last, 1)


    def arrived(g, side=None):
        for o, (i, device) in enumerate(peers):
            back_copy(o, i, device, g, i, side).wait_recv()

    def lines_of(g):
        return r.back[:, g].reshape(experts * 2 * SLOTS, width)

    def weighed(token_chip, side, g):
        code, share = slot_codes(r.aux_all[token_chip], z, experts)
        flat = jnp.where(slot_matches(code, side), share[:, None, :], 0.0)
        flat = flat.reshape(experts * 2 * SLOTS, tokens)
        return jnp.dot(flat.T.astype(BF16), lines_of(g), preferred_element_type=F32)

    def sum_ring(way, s, c):
        at = pl.ds(c * part, part)
        return remote(
            r.sums.at[way, s - 2, at],
            r.held.at[way, s - 2, at],
            r.sum_send.at[way, s - 2, c],
            r.sum_recv.at[way, s - 2, c],
            hop_to[way],
        )

    def part_of(c):
        return slice(c * part, (c + 1) * part)

    def target(way, s):
        return lax.rem(z + hops - s, nz) if way == 0 else lax.rem(z + nz - hops + s, nz)

    def from_far(way):
        picks, share = far_codes(1 - way)
        flat = jnp.where(picks, share, 0.0).reshape(many, tokens)
        lines = r.raw_in[1 - way].reshape(many, width)
        return jnp.dot(flat.T.astype(BF16), lines, preferred_element_type=F32)

    arrived(last - 2)
    near = [weighed(target(way, 2), 1 - way, last - 2) for way in (0, 1)]
    for way in (0, 1):
        for n in range(experts + nx):
            raw_arrival(1 - way, n).wait_recv()
        summed = near[way] + from_far(way)
        r.sums[way, 0] = summed.astype(BF16)
        for c in range(CHUNKS):
            sum_ring(way, 2, c).start()

    @pl.loop(3, hops)
    def _(s):
        g = last - s

        @pl.when(g > 1)
        def _():
            give_back(g - 2)

        arrived(g)
        mine = [weighed(target(way, s), 1 - way, g) for way in (0, 1)]
        for c in range(CHUNKS):
            for way in (0, 1):
                sum_ring(way, s - 1, c).wait_recv()
                summed = mine[way][part_of(c), :] + r.held[way, s - 3, part_of(c), :].astype(F32)
                r.sums[way, s - 2, part_of(c), :] = summed.astype(BF16)
                sum_ring(way, s, c).start()

    arrived(last, 1)
    code, share = slot_codes(r.aux_all[z], z, experts)
    slot = lax.broadcasted_iota(jnp.int32, (experts, SLOTS, tokens), 1).astype(F32)
    flat = jnp.where(code[:, None, :] == slot, share[:, None, :], 0.0)
    r.base[...] += jnp.dot(
        flat.reshape(experts * SLOTS, tokens).T.astype(BF16),
        r.back[:, last, SLOTS:].reshape(experts * SLOTS, width),
        preferred_element_type=F32,
    )
    for c in range(CHUNKS):
        for way in (0, 1):
            sum_ring(way, last, c).wait_recv()
        summed = (
            r.base[part_of(c), :]
            + r.held[0, last - 2, part_of(c), :].astype(F32)
            + r.held[1, last - 2, part_of(c), :].astype(F32)
        )
        r.out[part_of(c), :] = norm(summed, r.gain2[...], r.bias2[...]).astype(r.out.dtype)


    for o in range(1, nx):
        wo_copy(o, x).wait_send()
        head_copy(o, x, x).wait_send()
    for c in range(4):
        own_pair(c, sp).wait_send()

    @pl.loop(0, last)
    def _(s):
        for way in (0, 1):
            aux_hop(way, s, z).wait_send()
            for c in range(4):
                ring(way, s, c, sp).wait_send()
                pair(way, s, c, sp).wait_send()

    aux_hop(0, last, z).wait_send()
    for c in range(4):
        ring(c // 2, last, c, sp).wait_send()
        pair(c // 2, last, c, sp).wait_send()

    @pl.loop(0, last - 1)
    def _(s):
        for way in (0, 1):
            for c in range(CHUNKS):
                row_ring(way, s, c, z).wait_send()
                sum_ring(way, s + 2, c).wait_send()

    for way in (0, 1):
        for n in range(experts + nx):
            far_send(way, n).wait_send()
    for row in range(3):
        for i in range(experts):
            far_return(row, i).wait_send()
    slots_sent(last - 3)
    slots_sent(last - 2)
    for o, (i, device) in enumerate(peers):
        slot_copy(o, i, device, last, i, 1).wait_send()
        back_copy(o, i, device, last, i, 1).wait_send()

    @pl.loop(0, last - 1)
    def _(g):
        for o, (i, device) in enumerate(peers):
            back_copy(o, i, device, g, i).wait_send()


REFS = (
    "q",
    "k",
    "v",
    "wo",
    "aux",
    "res",
    "gain1",
    "bias1",
    "gain2",
    "bias2",
    "gate_hbm",
    "up_hbm",
    "down_hbm",
    "sgate_hbm",
    "sup_hbm",
    "sdown_hbm",
    "out",
    "kv",
    "acc",
    "behind",
    "far",
    "aux_all",
    "wo_all",
    "att",
    "heads",
    "rows_all",
    "base",
    "outgoing",
    "slots",
    "back",
    "gate",
    "up",
    "down",
    "sgate",
    "sup",
    "sdown",
    "far_out",
    "raw_in",
    "sums",
    "held",
    "load_sem",
    "kv_send",
    "kv_recv",
    "pair_send",
    "pair_recv",
    "own_send",
    "own_recv",
    "aux_send",
    "aux_recv",
    "wo_send",
    "wo_recv",
    "head_send",
    "head_recv",
    "row_send",
    "row_recv",
    "slot_send",
    "slot_recv",
    "back_send",
    "back_recv",
    "far_send",
    "far_recv",
    "raw_send",
    "raw_recv",
    "sum_send",
    "sum_recv",
)


def layer(nz, nx, q, k, v, wo, aux, res, norms, weights, shared):
    rows, head = q.shape
    tokens, width = res.shape
    hops = nz // 2
    experts = 2 * nx
    whole = pl.BlockSpec(memory_space=pltpu.VMEM)
    anywhere = pl.BlockSpec(memory_space=pl.ANY)
    dma = pltpu.SemaphoreType.DMA
    slot_shape = (experts, hops, 2 * SLOTS, width)
    return pl.pallas_call(
        functools.partial(layer_kernel, nz, nx),
        name="layer",
        out_shape=jax.ShapeDtypeStruct((tokens, width), BF16),
        in_specs=[whole] * 10 + [anywhere] * 6,
        out_specs=whole,
        scratch_shapes=[
            pltpu.VMEM((2, 2 * nz, rows, head), BF16),
            pltpu.VMEM((rows, head), F32),
            pltpu.VMEM((rows, KBLK), F32),
            pltpu.VMEM((rows, head), F32),
            pltpu.VMEM((nz, *aux.shape), F32),
            pltpu.VMEM((nx * wo.shape[0], width), BF16),
            pltpu.VMEM((rows, head), BF16),
            pltpu.VMEM((nx, tokens, head), BF16),
            pltpu.VMEM((nz, tokens, width), BF16),
            pltpu.VMEM((tokens, width), F32),
            pltpu.VMEM((experts, 3, 2 * SLOTS, width), BF16),
            pltpu.VMEM(slot_shape, BF16),
            pltpu.VMEM(slot_shape, BF16),
            *[pltpu.VMEM(w.shape, BF16) for w in (*weights, *shared)],
            pltpu.VMEM((2, experts + nx, SLOTS, width), BF16),
            pltpu.VMEM((2, experts + nx, SLOTS, width), BF16),
            pltpu.VMEM((2, hops - 2, tokens, width), BF16),
            pltpu.VMEM((2, hops - 2, tokens, width), BF16),
            dma((6,)),
            dma((2, hops, 4)),
            dma((2, hops, 4)),
            dma((2, hops, 4)),
            dma((2, hops, 4)),
            dma((4,)),
            dma((4,)),
            dma((2, hops)),
            dma((2, hops)),
            dma((nx - 1,)),
            dma((nx - 1,)),
            dma((nx - 1,)),
            dma((nx - 1,)),
            dma((2, hops - 2, CHUNKS)),
            dma((2, hops - 2, CHUNKS)),
            dma((experts - 1, hops + 1)),
            dma((experts - 1, hops + 1)),
            dma((experts - 1, hops)),
            dma((experts - 1, hops)),
            dma((2, experts + nx)),
            dma((3, experts)),
            dma((3, experts)),
            dma((2, experts + nx)),
            dma((2, hops - 2, CHUNKS)),
            dma((2, hops - 2, CHUNKS)),
        ],
        compiler_params=pltpu.CompilerParams(
            collective_id=0, has_side_effects=True, vmem_limit_bytes=67_000_000
        ),
        cost_estimate=pl.CostEstimate(flops=1 << 34, bytes_accessed=1 << 24, transcendentals=0),
    )(q, k, v, wo, aux, res, *norms, *weights, *shared)


def local(
    query_rows,
    key_rows,
    value_rows,
    residual,
    output_weight,
    first_gain,
    first_bias,
    expert_ids,
    expert_share,
    gate_weight,
    up_weight,
    down_weight,
    shared_gate,
    shared_up,
    shared_down,
    second_gain,
    second_bias,
):
    nz = lax.axis_size("sp") // 2
    nx = lax.axis_size("tp")
    aux = jnp.concatenate([expert_ids.T.astype(F32), expert_share.T], axis=0)
    norms = [a[None, :] for a in (first_gain, first_bias, second_gain, second_bias)]
    return layer(
        nz,
        nx,
        query_rows,
        key_rows,
        value_rows,
        output_weight,
        aux,
        residual,
        norms,
        (gate_weight, up_weight, down_weight),
        (shared_gate, shared_up, shared_down),
    )


def solution(mesh):
    return jax.shard_map(
        local,
        mesh=mesh,
        in_specs=(
            P(("grp", "sp"), "tp"),
            P(("grp", "sp"), "tp"),
            P(("grp", "sp"), "tp"),
            P(("grp", "sp", "tp"), None),
            P("tp", None),
            P(),
            P(),
            P(("grp", "sp", "tp"), None),
            P(("grp", "sp", "tp"), None),
            P(("sp", "tp"), None, None),
            P(("sp", "tp"), None, None),
            P(("sp", "tp"), None, None),
            P(),
            P(),
            P(),
            P(),
            P(),
        ),
        out_specs=P(("grp", "sp", "tp"), None),
        check_vma=False,
    )
```

time: 938 us -> 277 us (0.30)
  blocking collectives: 525 us -> 0 us
  waiting for transfers between devices: 273 us -> 0 us
  Pallas kernels: 0 us -> 272 us
  local copies, waits for them, and re-layouts: 58.8 us -> 1.88 us
  matrix products: 31.8 us -> 0 us
  starting transfers between devices: 20.3 us -> 0 us
  between operations: 13.6 us -> 0.01 us
    all_to_all x1 -> x0, blocking collectives: 525 us -> none  [local(): lax.all_to_all(outgoing, ('sp', 'tp'), split_axis=0, concat_axis=0, tiled...]
    pallas_call x0 -> x1, Pallas kernels: none -> 272 us  [layer(): pl.pallas_call(functools.partial(layer_kernel, nz, nx), name='layer', out...]
    all_to_all x3 -> x0, waiting for transfers between devices: 189 us -> none  [the longest x1 184 us: local(): lax.all_to_all(results, ('sp', 'tp'), split_axis=0, concat_axis=0, tiled=...]
    all_gather x1 -> x0, waiting for transfers between devices: 84.1 us -> none  [in_one_piece(): lax.all_gather(both, axis, axis=dim, tiled=True)]
    dot_general x10 -> x0, matrix products: 31.8 us -> none  [the longest x1 7.81 us: local(): jnp.dot(hidden, down_weight[0], preferred_element_type=jnp.float32)]
    reshape x7 -> x0, local copies, waits for them, and re-layouts: 30.9 us -> none  [the longest x1 6.34 us: local(): flat_rows = slot_rows.reshape(-1, width)]
    all_to_all x3 -> x0, starting transfers between devices: 20.3 us -> none  [the longest x1 11.1 us: local(): lax.all_to_all(results, ('sp', 'tp'), split_axis=0, concat_axis=0, tiled=...]
    gather x2 -> x0, local copies, waits for them, and re-layouts: 11.7 us -> none  [local(): jnp.take(flat_back, slot_ids, axis=0).reshape(tokens_here, top_count, width)]
  transfers between devices with their start and end apart: 4 -> 0, of which waited for: 3 -> 0; matrix products, arithmetic and copies ran while one was open for 4% -> 0% of each run, Pallas kernels for 0% -> 0%
where the time goes in v2:
time: 277 us; the launch traced here: 276 us
  Pallas kernels  272 us (98%)
    pallas_call x1, Pallas kernels, layer(): pl.pallas_call(functools.partial(layer_kernel, nz, nx), name='layer', out...  272 us

profile of v2, /device:TPU:33, one launch (start us, length us, event | category | flops | bytes accessed | tf_op | source)
XLA Modules:
  0.0 276.1 jit_solution(694241897377958453)
XLA Ops:
  0.0 0.7 convert_bitcast_fusion
  0.7 1.3 pad_maximum_fusion.refs_4_
  2.0 272.3 %layer.1 = bf16[128,2048]{1,0:T(8,128)(2,1)} custom-call(bf16[512,128]{1,0:T(8,128)(2,1)} %refs_0_.1, bf16[512,128]{1,0:T(8,128)(2,1)} %refs_1_.1, bf16[512,128]{1,0:T(8,128)(2,1)} %refs_2_.1, bf16[128,2048]{1,0:T(8,128)(2,1)} %refs_3_.1, f32[8,128]{1,0:T(8,128)} %pad_maximum_fusion.refs_4_, bf16[128,2048]{1,0:T(8,128)(2,1)} %refs_5_.1, f32[1,2048]{1,0:T(1,128)} %bitcast.8, ...), custom_call_target="tpu_custom_call" | custom-call | flops 17179869184 | bytes 16777216 | tf_op jit(solution)/shard_map/layer/pallas_call | solution.py:779
  274.2 1.9 copy.19

commit v3 on v2

--- a/solution.py
+++ b/solution.py
@@ -195,8 +195,6 @@
             across[o - 1],
         )
 
-    for way in (0, 1):
-        aux_hop(way, 0, z, r.aux).start()
     for c in range(4):
         for way in (0, 1):
             ring(way, 0, c, sp, own_piece(c)).start()
@@ -205,91 +203,89 @@
         wo_copy(o, x).start()
     for load in loads:
         load.start()
-
+    named = jnp.concatenate([r.ids[...].astype(F32), r.share[...]], axis=1)
+    r.aux_all[z] = named.T
     r.kv[0, sp] = r.k[...]
     r.kv[1, sp] = r.v[...]
-    r.aux_all[z] = r.aux[...]
     r.wo_all[pl.ds(x * wo_rows, wo_rows), :] = r.wo[...]
     r.acc[...] = jnp.zeros_like(r.acc)
     r.behind[...] = jnp.zeros_like(r.behind)
     r.far[...] = jnp.zeros_like(r.far)
-
-    tile = min(256, rows)
-    above = lax.broadcasted_iota(jnp.int32, (KBLK, 2 * KBLK), 0)
-    below = lax.broadcasted_iota(jnp.int32, (KBLK, 2 * KBLK), 1)
-    sums = ((above > below) | (below >= KBLK)).astype(F32).astype(BF16)
+    for way in (0, 1):
+        aux_hop(way, 0, z).start()
+
+    span = 2 * KBLK
+    above = lax.broadcasted_iota(jnp.int32, (span, span), 0)
+    below = lax.broadcasted_iota(jnp.int32, (span, span), 1)
+    later_keys = (above > below).astype(F32).astype(BF16)
     to_log2 = HEAD_DIM ** (-0.5) * LOG2E
 
-    def visit(block, mode):
-        @pl.loop(0, rows // tile)
-        def _(t):
-            here = pl.ds(pl.multiple_of(t * tile, tile), tile)
-            q = r.q[here, :]
-            spent_after = (
-                jnp.zeros((tile, KBLK), F32) if mode == "far" else r.behind[here, :]
+    def visit(first, blocks, mode):
+        q = r.q[...]
+        spent_after = jnp.zeros((rows, KBLK), F32) if mode == "far" else r.behind[...]
+        total = jnp.zeros((rows, HEAD_DIM), F32)
+        for b in reversed(range(blocks * rows // span)):
+            block = first + b * span // rows
+            at = pl.ds(b * span % rows, span)
+            score = (
+                lax.dot_general(
+                    q,
+                    r.kv[0, block, at, :],
+                    (((1,), (1,)), ((), ())),
+                    preferred_element_type=F32,
+                )
+                * to_log2
             )
-            total = jnp.zeros((tile, HEAD_DIM), F32)
-            for b in reversed(range(rows // KBLK)):
-                span = pl.ds(b * KBLK, KBLK)
-                score = (
-                    lax.dot_general(
-                        q,
-                        r.kv[0, block, span, :],
-                        (((1,), (1,)), ((), ())),
-                        preferred_element_type=F32,
-                    )
-                    * to_log2
-                )
-                soft = jnp.maximum(
-                    score, jnp.log(1.0 + jnp.exp2(jnp.minimum(score, 64.0))) * LOG2E
-                )
-                if mode == "diagonal":
-                    key_pos = b * KBLK + lax.broadcasted_iota(jnp.int32, (tile, KBLK), 1)
-                    query_pos = t * tile + lax.broadcasted_iota(jnp.int32, (tile, KBLK), 0)
-                    usable = key_pos < query_pos
-                    spent = jnp.where(usable, soft, 0.0)
-                else:
-                    spent = soft
-                added = jnp.dot(spent.astype(BF16), sums, preferred_element_type=F32)
-                weight = jnp.exp2(((score - soft) - added[:, :KBLK]) - spent_after)
-                if mode == "diagonal":
-                    weight = jnp.where(usable, weight, 0.0)
-                spent_after = spent_after + added[:, KBLK:]
-                total = total + jnp.dot(
-                    weight.astype(BF16), r.kv[1, block, span, :], preferred_element_type=F32
-                )
-            if mode == "far":
-                r.far[here, :] = r.far[here, :] * jnp.exp2(-spent_after) + total
+            soft = jnp.maximum(
+                score, jnp.log(1.0 + jnp.exp2(jnp.minimum(score, 64.0))) * LOG2E
+            )
+            if mode == "diagonal":
+                key_pos = b * span + lax.broadcasted_iota(jnp.int32, (rows, span), 1)
+                query_pos = lax.broadcasted_iota(jnp.int32, (rows, span), 0)
+                usable = key_pos < query_pos
+                spent = jnp.where(usable, soft, 0.0)
             else:
-                r.acc[here, :] = r.acc[here, :] + total
-                r.behind[here, :] = spent_after
-
-    def work(s, c):
-        near_chip = z - (s + 1)
-        far_chip = z + s + 1 - nz
-        if c < 2:
-
-            @pl.when(near_chip >= 0)
-            def _():
-                visit(jnp.maximum(2 * near_chip + 1 - c, 0), "near")
-
+                spent = soft
+            added = jnp.dot(spent.astype(BF16), later_keys, preferred_element_type=F32)
+            both = jnp.concatenate([spent_after] * (span // KBLK), axis=1)
+            weight = jnp.exp2(((score - soft) - added) - both)
+            if mode == "diagonal":
+                weight = jnp.where(usable, weight, 0.0)
+            spent_after = spent_after + (added[:, :1] + spent[:, :1])
+            total = total + jnp.dot(
+                weight.astype(BF16), r.kv[1, block, at, :], preferred_element_type=F32
+            )
+        if mode == "far":
+            r.far[...] = r.far[...] * jnp.exp2(-spent_after) + total
         else:
-
-            @pl.when(far_chip >= 0)
-            def _():
-                visit(jnp.maximum(2 * far_chip + c - 2, 0), "far")
+            r.acc[...] = r.acc[...] + total
+            r.behind[...] = spent_after
+
+    def work_near(s):
+        chip = z - (s + 1)
+
+        @pl.when(chip >= 0)
+        def _():
+            visit(jnp.maximum(2 * chip, 0), 2, "near")
+
+    def work_far(s):
+        chip = z + s + 1 - nz
+
+        @pl.when(chip >= 0)
+        def _():
+            visit(jnp.maximum(2 * chip, 0), 2, "far")
 
     def of_pair(way, s):
         return 2 * source(way, s) + 1 - core
 
-    visit(sp, "diagonal")
+    visit(sp, 1, "diagonal")
     other = sp + 1 - 2 * core
     for c in range(4):
         own_pair(c, other).wait_recv()
 
     @pl.when(core == 1)
     def _():
-        visit(other, "near")
+        visit(other, 1, "near")
 
     @pl.loop(0, last)
     def _(s):
@@ -314,19 +310,18 @@
 
                 pair(way, s, c, block).start()
 
-            @pl.when(s > 0)
-            def _():
-                if c == 0:
-                    for way in (0, 1):
-                        for c2 in range(4):
-                            pair(way, s - 1, c2, of_pair(way, s - 1)).wait_recv()
-                work(s - 1, c)
+            if c % 2 == 0:
+
+                @pl.when(s > 0)
+                def _():
+                    for c2 in range(4):
+                        pair(c // 2, s - 1, c2, of_pair(c // 2, s - 1)).wait_recv()
+                    (work_near, work_far)[c // 2](s - 1)
 
     for way in (0, 1):
         for c2 in range(4):
             pair(way, last - 1, c2, of_pair(way, last - 1)).wait_recv()
-    for c in range(4):
-        work(last - 1, c)
+        (work_near, work_far)[way](last - 1)
     aux_hop(0, last, source(0, last)).wait_recv()
     for c in range(4):
         way = c // 2
@@ -336,8 +331,7 @@
     for c in range(4):
         way = c // 2
         pair(way, last, c, of_pair(way, last)).wait_recv()
-    for c in range(2):
-        work(last, c)
+    work_near(last)
     r.att[...] = (r.acc[...] + r.far[...] * jnp.exp2(-r.behind[...])).astype(BF16)
 
 
@@ -703,7 +697,8 @@
     "k",
     "v",
     "wo",
-    "aux",
+    "ids",
+    "share",
     "res",
     "gain1",
     "bias1",
@@ -767,7 +762,7 @@
 )
 
 
-def layer(nz, nx, q, k, v, wo, aux, res, norms, weights, shared):
+def layer(nz, nx, q, k, v, wo, ids, share, res, norms, weights, shared):
     rows, head = q.shape
     tokens, width = res.shape
     hops = nz // 2
@@ -780,14 +775,14 @@
         functools.partial(layer_kernel, nz, nx),
         name="layer",
         out_shape=jax.ShapeDtypeStruct((tokens, width), BF16),
-        in_specs=[whole] * 10 + [anywhere] * 6,
+        in_specs=[whole] * 11 + [anywhere] * 6,
         out_specs=whole,
         scratch_shapes=[
             pltpu.VMEM((2, 2 * nz, rows, head), BF16),
             pltpu.VMEM((rows, head), F32),
             pltpu.VMEM((rows, KBLK), F32),
             pltpu.VMEM((rows, head), F32),
-            pltpu.VMEM((nz, *aux.shape), F32),
+            pltpu.VMEM((nz, 2 * ids.shape[1], tokens), F32),
             pltpu.VMEM((nx * wo.shape[0], width), BF16),
             pltpu.VMEM((rows, head), BF16),
             pltpu.VMEM((nx, tokens, head), BF16),
@@ -831,7 +826,7 @@
             collective_id=0, has_side_effects=True, vmem_limit_bytes=67_000_000
         ),
         cost_estimate=pl.CostEstimate(flops=1 << 34, bytes_accessed=1 << 24, transcendentals=0),
-    )(q, k, v, wo, aux, res, *norms, *weights, *shared)
+    )(q, k, v, wo, ids, share, res, *norms, *weights, *shared)
 
 
 def local(
@@ -855,7 +850,6 @@
 ):
     nz = lax.axis_size("sp") // 2
     nx = lax.axis_size("tp")
-    aux = jnp.concatenate([expert_ids.T.astype(F32), expert_share.T], axis=0)
     norms = [a[None, :] for a in (first_gain, first_bias, second_gain, second_bias)]
     return layer(
         nz,
@@ -864,7 +858,8 @@
         key_rows,
         value_rows,
         output_weight,
-        aux,
+        expert_ids,
+        expert_share,
         residual,
         norms,
         (gate_weight, up_weight, down_weight),

time: 277 us -> 268 us (0.968)
  Pallas kernels: 272 us -> 263 us
  local copies, waits for them, and re-layouts: 1.88 us -> 4.7 us
    pallas_call x1, Pallas kernels: 272 us -> 263 us  [layer(): pl.pallas_call(functools.partial(layer_kernel, nz, nx), name='layer', out...]
    unnamed x1 -> x3, local copies, waits for them, and re-layouts: 1.88 us -> 4.7 us
where the time goes in v3:
time: 268 us
  Pallas kernels  263 us (98%)
  local copies, waits for them, and re-layouts  4.7 us (2%)
    pallas_call x1, Pallas kernels, layer(): pl.pallas_call(functools.partial(layer_kernel, nz, nx), name='layer', out...  263 us

profile of v3, /device:TPU:33, one launch (start us, length us, event | category | flops | bytes accessed | tf_op | source)
XLA Modules:
  0.0 268.1 jit_solution(1455473572462632903)
XLA Ops:
  0.0 1.4 copy.18.refs_4_
  1.4 1.4 copy.19.refs_5_
  2.8 263.4 %layer.1 = bf16[128,2048]{1,0:T(8,128)(2,1)} custom-call(bf16[512,128]{1,0:T(8,128)(2,1)} %refs_0_.1, bf16[512,128]{1,0:T(8,128)(2,1)} %refs_1_.1, bf16[512,128]{1,0:T(8,128)(2,1)} %refs_2_.1, bf16[128,2048]{1,0:T(8,128)(2,1)} %refs_3_.1, s32[128,4]{1,0:T(8,128)} %copy.18.refs_4_, f32[128,4]{1,0:T(8,128)} %copy.19.refs_5_, bf16[128,2048]{1,0:T(8,128)(2,1)} %refs_6_.1, ...), custom_call_target="tpu_custom_call" | custom-call | flops 17179869184 | bytes 16777216 | tf_op jit(solution)/shard_map/layer/pallas_call | solution.py:774
  266.2 1.9 copy.21

commit v4 on v3

--- a/solution.py
+++ b/solution.py
@@ -112,6 +112,21 @@
     def member(chip, i):
         return {"sp": 2 * chip + i // nx, "tp": i % nx}
 
+    heads_at = pl.ds(x * r.wo_hbm.shape[0], r.wo_hbm.shape[0])
+    first_loads = [
+        pltpu.make_async_copy(src, dst, r.first_sem.at[n])
+        for n, (src, dst) in enumerate(
+            (
+                (r.k_hbm, r.kv.at[0, sp]),
+                (r.v_hbm, r.kv.at[1, sp]),
+                (r.q_hbm, r.q),
+                (r.wo_hbm, r.wo_all.at[heads_at]),
+                (r.res_hbm, r.res),
+            )
+        )
+    ]
+    for load in first_loads:
+        load.start()
     r.raw_in[...] = jnp.zeros_like(r.raw_in)
     greet(
         [device for _, device in peers]
@@ -148,17 +163,14 @@
 
 
     half = rows // 2
-    wo_rows = r.wo.shape[0]
+    wo_rows = r.wo_hbm.shape[0]
 
     def piece(block, c):
         return r.kv.at[c // 2, block, pl.ds((c % 2) * half, half)]
 
-    def own_piece(c):
-        return (r.k, r.v)[c // 2].at[pl.ds((c % 2) * half, half)]
-
-    def ring(way, s, c, block, src=None):
-        return remote(
-            piece(block, c) if src is None else src,
+    def ring(way, s, c, block):
+        return remote(
+            piece(block, c),
             piece(block, c),
             r.kv_send.at[way, s, c],
             r.kv_recv.at[way, s, c],
@@ -175,7 +187,7 @@
         )
 
     def own_pair(c, block):
-        return remote(own_piece(c), piece(block, c), r.own_send.at[c], r.own_recv.at[c], partner)
+        return remote(piece(block, c), piece(block, c), r.own_send.at[c], r.own_recv.at[c], partner)
 
     def aux_hop(way, s, block, src=None):
         return remote(
@@ -188,7 +200,7 @@
 
     def wo_copy(o, at):
         return remote(
-            r.wo,
+            r.wo_all.at[pl.ds(at * wo_rows, wo_rows)],
             r.wo_all.at[pl.ds(at * wo_rows, wo_rows)],
             r.wo_send.at[o - 1],
             r.wo_recv.at[o - 1],
@@ -196,18 +208,18 @@
         )
 
     for c in range(4):
+        if c % 2 == 0:
+            first_loads[c // 2].wait()
         for way in (0, 1):
-            ring(way, 0, c, sp, own_piece(c)).start()
+            ring(way, 0, c, sp).start()
         own_pair(c, sp).start()
+    for load in first_loads[2:]:
+        load.wait()
     for o in range(1, nx):
         wo_copy(o, x).start()
     for load in loads:
         load.start()
-    named = jnp.concatenate([r.ids[...].astype(F32), r.share[...]], axis=1)
-    r.aux_all[z] = named.T
-    r.kv[0, sp] = r.k[...]
-    r.kv[1, sp] = r.v[...]
-    r.wo_all[pl.ds(x * wo_rows, wo_rows), :] = r.wo[...]
+    r.aux_all[z] = jnp.concatenate([r.ids[...].astype(F32), r.share[...]], axis=0)
     r.acc[...] = jnp.zeros_like(r.acc)
     r.behind[...] = jnp.zeros_like(r.behind)
     r.far[...] = jnp.zeros_like(r.far)
@@ -693,13 +705,13 @@
 
 
 REFS = (
-    "q",
-    "k",
-    "v",
-    "wo",
+    "q_hbm",
+    "k_hbm",
+    "v_hbm",
+    "wo_hbm",
     "ids",
     "share",
-    "res",
+    "res_hbm",
     "gain1",
     "bias1",
     "gain2",
@@ -711,6 +723,8 @@
     "sup_hbm",
     "sdown_hbm",
     "out",
+    "q",
+    "res",
     "kv",
     "acc",
     "behind",
@@ -734,6 +748,7 @@
     "raw_in",
     "sums",
     "held",
+    "first_sem",
     "load_sem",
     "kv_send",
     "kv_recv",
@@ -775,14 +790,16 @@
         functools.partial(layer_kernel, nz, nx),
         name="layer",
         out_shape=jax.ShapeDtypeStruct((tokens, width), BF16),
-        in_specs=[whole] * 11 + [anywhere] * 6,
+        in_specs=[anywhere] * 4 + [whole] * 2 + [anywhere] + [whole] * 4 + [anywhere] * 6,
         out_specs=whole,
         scratch_shapes=[
+            pltpu.VMEM((rows, head), BF16),
+            pltpu.VMEM((tokens, width), BF16),
             pltpu.VMEM((2, 2 * nz, rows, head), BF16),
             pltpu.VMEM((rows, head), F32),
             pltpu.VMEM((rows, KBLK), F32),
             pltpu.VMEM((rows, head), F32),
-            pltpu.VMEM((nz, 2 * ids.shape[1], tokens), F32),
+            pltpu.VMEM((nz, 2 * ids.shape[0], tokens), F32),
             pltpu.VMEM((nx * wo.shape[0], width), BF16),
             pltpu.VMEM((rows, head), BF16),
             pltpu.VMEM((nx, tokens, head), BF16),
@@ -796,6 +813,7 @@
             pltpu.VMEM((2, experts + nx, SLOTS, width), BF16),
             pltpu.VMEM((2, hops - 2, tokens, width), BF16),
             pltpu.VMEM((2, hops - 2, tokens, width), BF16),
+            dma((5,)),
             dma((6,)),
             dma((2, hops, 4)),
             dma((2, hops, 4)),
@@ -858,8 +876,8 @@
         key_rows,
         value_rows,
         output_weight,
-        expert_ids,
-        expert_share,
+        expert_ids.T,
+        expert_share.T,
         residual,
         norms,
         (gate_weight, up_weight, down_weight),

time: 268 us -> 265 us (0.989)
  local copies, waits for them, and re-layouts: 4.7 us -> 1.88 us
    unnamed x3 -> x1, local copies, waits for them, and re-layouts: 4.7 us -> 1.88 us
where the time goes in v4:
time: 265 us
  Pallas kernels  263 us (99%)
    pallas_call x1, Pallas kernels, layer(): pl.pallas_call(functools.partial(layer_kernel, nz, nx), name='layer', out...  263 us

profile of v4, /device:TPU:33, one launch (start us, length us, event | category | flops | bytes accessed | tf_op | source)
XLA Modules:
  0.0 264.8 jit_solution(1437152139229004030)
XLA Ops:
  0.0 262.9 %layer.1 = bf16[128,2048]{1,0:T(8,128)(2,1)} custom-call(bf16[512,128]{1,0:T(8,128)(2,1)} %refs_0_.1, bf16[512,128]{1,0:T(8,128)(2,1)} %refs_1_.1, bf16[512,128]{1,0:T(8,128)(2,1)} %refs_2_.1, bf16[128,2048]{1,0:T(8,128)(2,1)} %refs_3_.1, s32[4,128]{1,0:T(4,128)} %bitcast.10, f32[4,128]{1,0:T(4,128)} %bitcast.11, bf16[128,2048]{1,0:T(8,128)(2,1)} %refs_6_.1, ...), custom_call_target="tpu_custom_call" | custom-call | flops 17179869184 | bytes 16777216 | tf_op jit(solution)/shard_map/layer/pallas_call | solution.py:789
  262.9 1.9 copy.19
